TPU v7x, 256 devices: a whole 4x4x8 slice. The times are simulated.
256 devices in a mesh: sp: 64 (over z, x, core), tp: 4 (over y).
Axes of the slice: x: 4, y: 4, z: 8, core: 2. Of those that a mesh axis runs over, the one named last changes fastest.
Arguments:
- hidden_in: bfloat16 [4096, 2048], P(('sp', 'tp')), may hold values from -6 to 6
- pre_gain: float32 [2048], replicated, may hold values from 0.5 to 1.5
- w_query: bfloat16 [2048, 1024], P(None, 'tp'), may hold values from -0.4375 to 0.4375
- w_key: bfloat16 [2048, 1024], P(None, 'tp'), may hold values from -0.125 to 0.125
- w_value: bfloat16 [2048, 1024], P(None, 'tp'), may hold values from -0.125 to 0.125
- stick_offset: float32 [8], P('tp'), may hold values from -15.2 to -14.2
- w_glu_a: bfloat16 [2048, 1024], P(None, 'tp'), may hold values from -0.125 to 0.125
- w_glu_b: bfloat16 [2048, 1024], P(None, 'tp'), may hold values from -0.125 to 0.125
- w_gate_attn: bfloat16 [2048, 2048], P(None, 'tp'), may hold values from -0.125 to 0.125
- w_gate_conv: bfloat16 [2048, 2048], P(None, 'tp'), may hold values from -0.125 to 0.125
- conv_taps: float32 [31, 1024], P(None, 'tp'), may hold values from -1 to 1
- conv_bias: float32 [1024], P('tp'), may hold values from -0.6 to 0.6
- norm_gain: float32 [1024], P('tp'), may hold values from 0.5 to 1.5
- norm_shift: float32 [1024], P('tp'), may hold values from -0.6 to 0.6
- w_attn_out: bfloat16 [1024, 2048], P('tp'), may hold values from -0.4375 to 0.4375
- w_conv_out: bfloat16 [1024, 2048], P('tp'), may hold values from -0.1875 to 0.1875
- post_gain: float32 [2048], P('tp'), may hold values from 0.5 to 1.5
Outputs:
- mixed: bfloat16 [4096, 2048], P('sp', 'tp')
All inputs are finite; a program needn't handle non-finite values.
Results may differ from a plain program's by a relative error of at most 0.015.
Values may be sent and summed in bfloat16 or wider, within the bound.
No kernel may reach another device: no remote copies, remote signals or barrier semaphores. Data moves between devices by JAX's collectives and lax.ppermute only.
A program may use at most 64 MiB of HBM per device.

v0:
```python
import math

import jax
import jax.numpy as jnp
from jax import lax
from jax.experimental import pallas as pl
from jax.experimental.pallas import tpu as pltpu
from jax.sharding import Mesh
from jax.sharding import PartitionSpec as P

D = 2048
HEAD_DIM = 128
CONV_CH = 1024
WIDTH = 31
HALO = 32
SP = ("zh", "zl", "x", "c")
SP_TP = ("zh", "zl", "x", "c", "tp")
N_ZH = 4
N_TP = 4
LOG2E = math.log2(math.e)
BF16 = jnp.bfloat16
F32 = jnp.float32
epsilon = 1e-06
MIB = 1024 * 1024
LOAD_PARTS = 4


def dot(a, b):
    return jnp.dot(a, b, preferred_element_type=F32)


def call(body, outs, args, scratch=(), vmem=8, flops=0, out_space=jax.ShapeDtypeStruct):
    spaces = {"smem": pltpu.SMEM, "vmem": pltpu.VMEM, "hbm": pltpu.HBM}
    specs = [pl.BlockSpec(memory_space=spaces[kind]) for kind, _ in args]
    return pallas_call(body, outs, specs, args, scratch, vmem, flops, out_space)


def pallas_call(body, outs, specs, args, scratch, vmem, flops, out_space):
    return pl.pallas_call(
        body,
        out_shape=[out_space(shape, dtype) for shape, dtype in outs],
        in_specs=specs,
        out_specs=[pl.BlockSpec(memory_space=pltpu.VMEM) for _ in outs],
        scratch_shapes=list(scratch),
        compiler_params=pltpu.CompilerParams(vmem_limit_bytes=vmem * MIB),
        cost_estimate=pl.CostEstimate(flops=flops, transcendentals=0, bytes_accessed=0),
    )(*[array for _, array in args])


def to_rotated(pieces):
    return [lax.ppermute(piece, "tp", [(i, (i + d) % N_TP) for i in range(N_TP)]) for d, piece in enumerate(pieces, 1)]


def load_body(*refs):
    count = (len(refs) - 1) // 2
    sems = refs[-1]
    copies = []
    for source, target in zip(refs[:count], refs[count:-1]):
        parts = LOAD_PARTS if source.shape[0] >= 256 else 1
        rows = source.shape[0] // parts
        for i in range(parts):
            part = pl.ds(i * rows, rows)
            copies.append(pltpu.make_async_copy(source.at[part], target.at[part], sems.at[len(copies)]))
    for copy in copies:
        copy.start()
    for copy in copies:
        copy.wait()


def loaded(arrays):
    arrays = [pltpu.with_memory_space_constraint(x, pltpu.HBM) for x in arrays]
    return call(
        load_body,
        [(x.shape, x.dtype) for x in arrays],
        [("hbm", x) for x in arrays],
        scratch=[pltpu.SemaphoreType.DMA((LOAD_PARTS * len(arrays),))],
        flops=10000000,
        out_space=pltpu.VMEM,
    )


def qkv_body(x0, x1, x2, x3, gain, wq, wk, wv, kv_out, q_out, normed_out, rows):
    me = lax.axis_index("tp")
    for d, ref in enumerate((x0, x1, x2, x3)):
        source = lax.rem(me + N_TP - d, N_TP)
        rows[pl.ds(pl.multiple_of(source * 16, 16), 16), :] = ref[...]
    values = rows[...].astype(F32)
    inverse = lax.rsqrt(jnp.mean(values * values, axis=1, keepdims=True) + epsilon)
    normed = (values * inverse * gain[...]).astype(BF16)
    normed_out[...] = normed
    keys = dot(normed, wk[...]).astype(BF16)
    vals = dot(normed, wv[...]).astype(BF16)
    for i in range(kv_out.shape[0]):
        kv_out[i, :, 0:256] = keys
        kv_out[i, :, 256:512] = vals
    q_out[...] = dot(normed, wq[...]).astype(BF16)


def glu_body(normed_ref, wa, wb, gated_out, tail_out):
    normed = normed_ref[...]
    left = dot(normed, wa[...]).astype(BF16).astype(F32)
    right = dot(normed, wb[...]).astype(BF16).astype(F32)
    gated = (left * jax.nn.sigmoid(right)).astype(BF16)
    gated_out[...] = gated
    tail_out[...] = gated[gated.shape[0] - HALO :, :]


def gates_body(normed_ref, wa, wc, ga_out, gc_out, held, sems):
    rows = D // LOAD_PARTS
    copies = []
    for i in range(LOAD_PARTS):
        part = pl.ds(i * rows, rows)
        for j, source in enumerate((wa, wc)):
            copies.append(pltpu.make_async_copy(source.at[part], held.at[j, part], sems.at[len(copies)]))
    for copy in copies:
        copy.start()
    totals = [0.0, 0.0]
    for i in range(LOAD_PARTS):
        part = slice(i * rows, i * rows + rows)
        for j in range(2):
            copies[2 * i + j].wait()
            totals[j] = totals[j] + dot(normed_ref[:, part], held[j, part, :])
    ga_out[...] = jax.nn.sigmoid(totals[0].astype(BF16).astype(F32))
    gc_out[...] = jax.nn.sigmoid(totals[1].astype(BF16).astype(F32))


def conv_body(gated_ref, tail_ref, taps, bias, conv_out, stat_out, padded):
    rows = gated_ref.shape[0]
    padded[0:HALO, :] = tail_ref[...].astype(F32)
    padded[HALO : HALO + rows, :] = gated_ref[...].astype(F32)
    total = jnp.broadcast_to(bias[...], (rows, bias.shape[1]))
    first = HALO - (WIDTH - 1)
    for i in range(WIDTH):
        total = total + taps[i : i + 1, :] * padded[first + i : first + i + rows, :]
    conv_out[...] = total
    mean = jnp.mean(total, axis=1, keepdims=True)
    centered = total - mean
    squares = jnp.sum(centered * centered, axis=1, keepdims=True)
    lane = lax.broadcasted_iota(jnp.int32, (rows, 128), 1)
    turned = jnp.transpose(jnp.where(lane < 4, mean, squares))
    stat_out[...] = turned[0:8, :]


def conv_norm_body(conv_ref, s0, s1, s2, s3, gain, shift, normed_out):
    stats = [s[...] for s in (s0, s1, s2, s3)]
    means = [s[0:4, :] for s in stats]
    mean = (means[0] + means[1] + means[2] + means[3]) * (1.0 / N_TP)
    spread = jnp.zeros_like(mean)
    for s, m in zip(stats, means):
        spread = spread + s[4:8, :] + (m - mean) * (m - mean) * (CONV_CH // N_TP)
    inverse = lax.rsqrt(spread * (1.0 / CONV_CH) + epsilon)
    columns = jnp.transpose(jnp.concatenate([mean, inverse], axis=0))
    mean = columns[:, 0:1]
    inverse = columns[:, 4:5]
    scaled = (conv_ref[...] - mean) * inverse * gain[...] + shift[...]
    normed_out[...] = (scaled * jax.nn.sigmoid(scaled)).astype(BF16)


def attend_body(offset, q0, q1, q2, q3, mine, other, acc_out, rest_out, m1, m2, m3):
    group = lax.axis_index("zh")
    visitors = ((q1, m1), (q2, m2), (q3, m3))
    for condition, count in ((group < N_ZH - 2, 3), (group == N_ZH - 2, 1), (group == N_ZH - 1, 0)):

        @pl.when(condition)
        def _():
            attend(offset, q0, visitors[:count], mine, other, acc_out, rest_out)


def attend(offset, q0, visitors, mine, other, acc_out, rest_out):
    core = lax.axis_index("c")
    rows = q0.shape[0]
    blocks = mine.shape[0]
    total_rows = rows * (1 + len(visitors))
    position = (lax.axis_index("zl") * 4 + lax.axis_index("x")) * 128 + core * 64
    query_pos = position + lax.broadcasted_iota(jnp.int32, (rows, 128), 0)
    index = lax.broadcasted_iota(jnp.int32, (1, 128), 1)
    place = lax.rem(index + core * 64, 128)
    row_index = lax.rem(lax.broadcasted_iota(jnp.int32, (256, 256), 0), 128)
    col_index = lax.broadcasted_iota(jnp.int32, (256, 256), 1)
    row_place = lax.rem(row_index + core * 64, 128)
    col_place = lax.rem(col_index + core * 64, 128)
    suffix = jnp.where((col_index >= 128) | (row_place >= col_place), 1.0, 0.0).astype(BF16)
    scale = LOG2E / math.sqrt(HEAD_DIM)

    tiles = range(blocks)
    span = [slice(b * 128, b * 128 + 128) for b in tiles]
    own_causal = [(b * 128 + place) < query_pos for b in tiles]

    def for_own(b, x):
        masked = jnp.where(own_causal[b], x[:rows], 0.0)
        return jnp.concatenate([masked, x[rows:]], axis=0) if visitors else masked

    for h in range(2):
        lanes = slice(h * 128, h * 128 + 128)
        value_lanes = slice(256 + h * 128, 256 + h * 128 + 128)
        queries = jnp.concatenate([q[:, lanes] for q in [q0] + [q for q, _ in visitors]], axis=0)
        keys = jnp.concatenate([ref[b, :, lanes] for b in tiles for ref in (mine, other)], axis=0)
        vals = jnp.concatenate([ref[b, :, value_lanes] for b in tiles for ref in (mine, other)], axis=0)
        scores = lax.dot_general(queries, keys, (((1,), (1,)), ((), ())), preferred_element_type=F32)
        scores = scores * scale + offset[h] * LOG2E
        soft = jnp.maximum(scores, 0.0) + jnp.log2(1.0 + jnp.exp2(-jnp.abs(scores)))
        split = []
        for b in tiles:
            part = for_own(b, soft[:, span[b]])
            high = part.astype(BF16)
            low = (part - high.astype(F32)).astype(BF16)
            split.append(jnp.concatenate([high, low], axis=1))
        sums = dot(jnp.concatenate(split, axis=0), suffix)
        sums = [sums[b * total_rows : (b + 1) * total_rows] for b in tiles]
        rest = jnp.zeros((total_rows, 128), F32)
        sticks = [None] * blocks
        for b in reversed(tiles):
            stick = for_own(b, jnp.exp2(scores[:, span[b]] - (sums[b][:, 0:128] + rest)))
            sticks[b] = stick.astype(BF16)
            rest = rest + sums[b][:, 128:256]
        acc = dot(jnp.concatenate(sticks, axis=1), vals)
        acc_out[:, lanes] = acc[:rows]
        rest_out[:, lanes] = rest[:rows]
        lane = lax.broadcasted_iota(jnp.int32, (rows, 64), 1)
        for d, (_, ref) in enumerate(visitors, 1):
            part = slice(d * rows, d * rows + rows)
            ref[:, lanes] = acc[part].astype(BF16)
            total = rest[part][:, 0:64]
            t1 = total.astype(BF16).astype(F32)
            t2 = (total - t1).astype(BF16).astype(F32)
            t3 = total - t1 - t2
            ref[:, 256 + h * 64 : 320 + h * 64] = jnp.where(lane == 0, t1, jnp.where(lane == 1, t2, t3)).astype(BF16)


def merge_body(acc_ref, rest_ref, m1, m2, m3, conv, w_attn, w_conv, own_out, p1, p2, p3):
    heads = []
    for h in range(2):
        lanes = slice(h * 128, h * 128 + 128)
        outside = rest_ref[:, lanes]
        total = acc_ref[:, lanes]
        for ref in (m1, m2, m3):
            total = total + jnp.exp2(-outside) * ref[:, lanes].astype(F32)
            sent = ref[:, 256 + h * 64 : 320 + h * 64].astype(F32)
            outside = outside + (sent[:, 0:1] + sent[:, 1:2] + sent[:, 2:3])
        heads.append(total.astype(BF16))
    attended = jnp.concatenate(heads, axis=1)
    convolved = conv[...]
    me = lax.axis_index("tp")
    width = own_out.shape[1] // 2
    for d, ref in enumerate((own_out, p1, p2, p3)):
        target = lax.rem(me + d, N_TP)
        columns = pl.ds(pl.multiple_of(target * width, width), width)
        ref[:, 0:width] = dot(attended, w_attn[:, columns]).astype(ref.dtype)
        ref[:, width : 2 * width] = dot(convolved, w_conv[:, columns]).astype(ref.dtype)


def gather_body(p0, p1, p2, p3, ga, gc, merged_out, stat_out):
    total = p0[...] + p1[...].astype(F32) + p2[...].astype(F32) + p3[...].astype(F32)
    branches = total.astype(BF16).astype(F32)
    width = branches.shape[1] // 2
    attn, conv = branches[:, :width], branches[:, width:]
    merged = ga[...] * attn + gc[...] * conv
    merged_out[...] = merged
    square = jnp.sum(merged * merged, axis=1, keepdims=True)
    stat_out[...] = jnp.transpose(jnp.broadcast_to(square, (square.shape[0], 128)))[0:8, :]


def final_body(merged, s0, s1, s2, s3, gain, out):
    squares = (s0[...] + s1[...] + s2[...] + s3[...]) * (1.0 / D)
    inverse = jnp.transpose(lax.rsqrt(squares + epsilon))[:, 0:1]
    out[...] = (merged[...] * inverse * gain[...]).astype(BF16)


def on_device(
    hidden_in,
    pre_gain,
    w_query,
    w_key,
    w_value,
    stick_offset,
    w_glu_a,
    w_glu_b,
    w_gate_attn,
    w_gate_conv,
    conv_taps,
    conv_bias,
    norm_gain,
    norm_shift,
    w_attn_out,
    w_conv_out,
    post_gain,
):
    def v(x):
        return ("vmem", x)

    rows = 64
    pieces = to_rotated([hidden_in] * 3)
    hidden, gain, wq, wk, wv, wga, wgb = loaded(
        (hidden_in, pre_gain.reshape(1, D), w_query, w_key, w_value, w_glu_a, w_glu_b)
    )
    wao, wco = loaded((w_attn_out, w_conv_out))
    kv, q, normed = call(
        qkv_body,
        [((8, rows, 512), BF16), ((rows, 256), BF16), ((rows, D), BF16)],
        [v(p) for p in [hidden] + pieces] + [v(gain), v(wq), v(wk), v(wv)],
        scratch=[pltpu.VMEM((rows, D), BF16)],
        flops=2 * rows * D * 768,
    )
    kv_mine = lax.all_to_all(kv, ("zl", "x"), 0, 0)
    visitors = [lax.ppermute(q, "zh", [(i, i - d) for i in range(d, N_ZH)]) for d in range(1, N_ZH)]
    gated, tail = call(
        glu_body, [((rows, 256), BF16), ((HALO, 256), BF16)], [v(normed), v(wga), v(wgb)], flops=2 * rows * D * 512
    )
    before = lax.ppermute(tail, SP, [(i, i + 1) for i in range(lax.axis_size(SP) - 1)])
    gate_a, gate_c = call(
        gates_body,
        [((rows, 512), F32), ((rows, 512), F32)],
        [v(normed)] + [("hbm", pltpu.with_memory_space_constraint(w, pltpu.HBM)) for w in (w_gate_attn, w_gate_conv)],
        scratch=[pltpu.VMEM((2, D, 512), BF16), pltpu.SemaphoreType.DMA((2 * LOAD_PARTS,))],
        flops=2 * rows * D * 1024,
    )
    convolved, stat = call(
        conv_body,
        [((rows, 256), F32), ((8, rows), F32)],
        [v(gated), v(before), v(conv_taps), v(conv_bias.reshape(1, 256))],
        scratch=[pltpu.VMEM((rows + HALO, 256), F32)],
        flops=2 * rows * 256 * 31 * 40,
    )
    stats = [stat] + to_rotated([stat] * 3)
    (conv_normed,) = call(
        conv_norm_body,
        [((rows, 256), BF16)],
        [v(convolved)]
        + [v(s) for s in stats]
        + [v(norm_gain.reshape(1, 256)), v(norm_shift.reshape(1, 256))],
        flops=2 * rows * 256 * 100,
    )
    kv_other = lax.ppermute(kv_mine, "c", [(0, 1), (1, 0)])
    acc, rest, *messages = call(
        attend_body,
        [((rows, 256), F32), ((rows, 256), F32)] + [((rows, 384), BF16)] * 3,
        [("smem", stick_offset), v(q)] + [v(x) for x in visitors] + [v(kv_mine), v(kv_other)],
        flops=2 * 2 * 256 * 1024 * 128 * 2,
    )
    returned = [lax.ppermute(m, "zh", [(i, i + d) for i in range(N_ZH - d)]) for d, m in enumerate(messages, 1)]
    partial = call(
        merge_body,
        [((rows, 1024), F32)] + [((rows, 1024), BF16)] * 3,
        [v(acc), v(rest)] + [v(m) for m in returned] + [v(conv_normed), v(wao), v(wco)],
        flops=4 * rows * 256 * D,
    )
    pieces = [partial[0]] + to_rotated(partial[1:])
    merged, square = call(
        gather_body,
        [((rows, 512), F32), ((8, rows), F32)],
        [v(x) for x in pieces] + [v(gate_a), v(gate_c)],
        flops=1000000,
    )
    squares = [square] + to_rotated([square] * 3)
    (out,) = call(
        final_body,
        [((rows, 512), BF16)],
        [v(merged)] + [v(s) for s in squares] + [v(post_gain.reshape(1, 512))],
        flops=1000000,
    )
    return out


def solution(mesh):
    torus = Mesh(mesh.devices.reshape(4, 2, 4, 2, mesh.shape["tp"]), SP_TP)

    return jax.shard_map(
        on_device,
        mesh=torus,
        in_specs=(
            P(SP_TP, None),
            P(),
            P(None, "tp"),
            P(None, "tp"),
            P(None, "tp"),
            P("tp"),
            P(None, "tp"),
            P(None, "tp"),
            P(None, "tp"),
            P(None, "tp"),
            P(None, "tp"),
            P("tp"),
            P("tp"),
            P("tp"),
            P("tp", None),
            P("tp", None),
            P("tp"),
        ),
        out_specs=P(SP, "tp"),
        check_vma=False,
    )
```

profile of v0, /device:TPU:32, one launch (start us, length us, event | category | flops | bytes accessed | tf_op | source)
XLA Modules:
  0.0 81.2 jit_solution(16233724931836692552)
XLA Ops:
  0.0 1.6 %collective-permute-start = (bf16[16,2048]{1,0:T(8,128)(2,1)}, bf16[16,2048]{1,0:T(8,128)(2,1)S(1)}, u32[]{:S(2)}, u32[]{:S(2)}) collective-permute-start(bf16[16,2048]{1,0:T(8,128)(2,1)} %refs_0_.2), channel_id=1, source_target_pairs={{0,1},{1,2},{2,3},{3,0},{4,5},{5,6},{6,7},{7,4},{8,9},{9,10},{10,1... | collective-permute-start | bytes 196616 | tf_op jit(solution)/shard_map/ppermute | solution.py:51
  1.6 2.9 %collective-permute-start.1 = (bf16[16,2048]{1,0:T(8,128)(2,1)}, bf16[16,2048]{1,0:T(8,128)(2,1)S(1)}, u32[]{:S(2)}, u32[]{:S(2)}) collective-permute-start(bf16[16,2048]{1,0:T(8,128)(2,1)} %refs_0_.2), channel_id=1, source_target_pairs={{0,2},{1,3},{2,0},{3,1},{4,6},{5,7},{6,4},{7,5},{8,10},{9,11},{10,... | collective-permute-start | bytes 196616 | tf_op jit(solution)/shard_map/ppermute | solution.py:51
  4.5 1.3 %collective-permute-start.2 = (bf16[16,2048]{1,0:T(8,128)(2,1)}, bf16[16,2048]{1,0:T(8,128)(2,1)S(1)}, u32[]{:S(2)}, u32[]{:S(2)}) collective-permute-start(bf16[16,2048]{1,0:T(8,128)(2,1)} %refs_0_.2), channel_id=1, source_target_pairs={{0,3},{1,0},{2,1},{3,2},{4,7},{5,4},{6,5},{7,6},{8,11},{9,8},{10,9... | collective-permute-start | bytes 196616 | tf_op jit(solution)/shard_map/ppermute | solution.py:51
  5.8 2.7 %shard_map.163 = (bf16[16,2048]{1,0:T(8,128)(2,1)S(1)}, f32[1,2048]{1,0:T(1,128)S(1)}, bf16[2048,256]{1,0:T(8,128)(2,1)S(1)}, bf16[2048,256]{1,0:T(8,128)(2,1)S(...) custom-call(bf16[16,2048]{1,0:T(8,128)(2,1)} %refs_0_.2, ...), custom_call_target="tpu_custom_call" | custom-call | flops 10000000 | tf_op jit(solution)/shard_map/pallas_call | solution.py:39
  8.6 0.0 collective-permute-done.x1
  8.6 0.0 collective-permute-done.1.x2
  8.6 0.4 collective-permute-done.2.x3
  9.0 0.8 shard_map.164
  9.8 0.0 copy-start.4
  9.8 0.0 copy-start.5
  9.8 13.1 %all_to_all.5.mine = bf16[8,64,512]{2,1,0:T(8,128)(2,1)S(1)} all-to-all(bf16[8,64,512]{2,1,0:T(8,128)(2,1)S(1)} %get-tuple-element.40), channel_id=1, replica_groups=mesh['zh'=4,'zl'=2,'x'=4,'c'=2,'tp'=4] {'zl','x'}, dimensions={0} | all-to-all | bytes 1048576 | tf_op jit(solution)/shard_map/all_to_all | solution.py:304
  22.9 1.3 %collective-permute-start.3 = (bf16[64,256]{1,0:T(8,128)(2,1)S(1)}, bf16[64,256]{1,0:T(8,128)(2,1)S(1)}, u32[]{:S(2)}, u32[]{:S(2)}) collective-permute-start(bf16[64,256]{1,0:T(8,128)(2,1)S(1)} %get-tuple-element.39.q0), channel_id=1, source_target_pairs={{64,0},{128,64},{192,128},{65,1},{129,65},{193,129},{66,2},{130,66... | collective-permute-start | bytes 98312 | tf_op jit(solution)/shard_map/ppermute | solution.py:305
  24.2 1.3 %collective-permute-start.4 = (bf16[64,256]{1,0:T(8,128)(2,1)S(1)}, bf16[64,256]{1,0:T(8,128)(2,1)S(1)}, u32[]{:S(2)}, u32[]{:S(2)}) collective-permute-start(bf16[64,256]{1,0:T(8,128)(2,1)S(1)} %get-tuple-element.39.q0), channel_id=1, source_target_pairs={{128,0},{192,64},{129,1},{193,65},{130,2},{194,66},{131,3},{195,67... | collective-permute-start | bytes 98312 | tf_op jit(solution)/shard_map/ppermute | solution.py:305
  25.5 1.3 %collective-permute-start.5 = (bf16[64,256]{1,0:T(8,128)(2,1)S(1)}, bf16[64,256]{1,0:T(8,128)(2,1)S(1)}, u32[]{:S(2)}, u32[]{:S(2)}) collective-permute-start(bf16[64,256]{1,0:T(8,128)(2,1)S(1)} %get-tuple-element.39.q0), channel_id=1, source_target_pairs={{192,0},{193,1},{194,2},{195,3},{196,4},{197,5},{198,6},{199,7},{2... | collective-permute-start | bytes 98312 | tf_op jit(solution)/shard_map/ppermute | solution.py:305
  26.8 3.3 %collective-permute-done.3.q1 = bf16[64,256]{1,0:T(8,128)(2,1)S(1)} collective-permute-done((bf16[64,256]{1,0:T(8,128)(2,1)S(1)}, bf16[64,256]{1,0:T(8,128)(2,1)S(1)}, u32[]{:S(2)}, u32[]{:S(2)}) %collective-permute-start.3) | collective-permute-done | bytes 32800 | tf_op jit(solution)/shard_map/ppermute | solution.py:305
  30.1 4.7 %collective-permute-done.4.q2 = bf16[64,256]{1,0:T(8,128)(2,1)S(1)} collective-permute-done((bf16[64,256]{1,0:T(8,128)(2,1)S(1)}, bf16[64,256]{1,0:T(8,128)(2,1)S(1)}, u32[]{:S(2)}, u32[]{:S(2)}) %collective-permute-start.4) | collective-permute-done | bytes 32800 | tf_op jit(solution)/shard_map/ppermute | solution.py:305
  34.9 2.8 %collective-permute-done.5.q3 = bf16[64,256]{1,0:T(8,128)(2,1)S(1)} collective-permute-done((bf16[64,256]{1,0:T(8,128)(2,1)S(1)}, bf16[64,256]{1,0:T(8,128)(2,1)S(1)}, u32[]{:S(2)}, u32[]{:S(2)}) %collective-permute-start.5) | collective-permute-done | bytes 32800 | tf_op jit(solution)/shard_map/ppermute | solution.py:305
  37.7 3.0 %shard_map.165 = (f32[64,256]{1,0:T(8,128)S(1)}, f32[64,256]{1,0:T(8,128)S(1)}, bf16[64,384]{1,0:T(8,128)(2,1)S(1)}, bf16[64,384]{1,0:T(8,128)(2,1)S(1)}, bf16[64,384]{1,0:T(8,128)(2,1)S(1)}) custom-call(f32[2]{0:T(128)S(1)} %copy-done.3, bf16[64,256]{1,0:T(8,128)(2,1)S(1)} %get-tuple-element.39.q0, bf16[64,256]{1,0:T(8,128)(2,1)S(1)} %collective-permute-done.3.q1, ...), custom_call_target="tpu_custom_call" | custom-call | flops 268435456 | tf_op jit(solution)/shard_map/pallas_call | solution.py:39
  40.7 2.0 %collective-permute-start.7 = (bf16[64,384]{1,0:T(8,128)(2,1)S(1)}, bf16[64,384]{1,0:T(8,128)(2,1)S(1)}, u32[]{:S(2)}, u32[]{:S(2)}) collective-permute-start(bf16[64,384]{1,0:T(8,128)(2,1)S(1)} %get-tuple-element.43), channel_id=1, source_target_pairs={{0,64},{64,128},{128,192},{1,65},{65,129},{129,193},{2,66},{66,130... | collective-permute-start | bytes 147464 | tf_op jit(solution)/shard_map/ppermute | solution.py:340
  42.6 2.2 %collective-permute-start.8 = (bf16[64,384]{1,0:T(8,128)(2,1)S(1)}, bf16[64,384]{1,0:T(8,128)(2,1)S(1)}, u32[]{:S(2)}, u32[]{:S(2)}) collective-permute-start(bf16[64,384]{1,0:T(8,128)(2,1)S(1)} %get-tuple-element.44), channel_id=1, source_target_pairs={{0,128},{64,192},{1,129},{65,193},{2,130},{66,194},{3,131},{67,195... | collective-permute-start | bytes 147464 | tf_op jit(solution)/shard_map/ppermute | solution.py:340
  44.8 1.3 %collective-permute-start.9 = (bf16[64,384]{1,0:T(8,128)(2,1)S(1)}, bf16[64,384]{1,0:T(8,128)(2,1)S(1)}, u32[]{:S(2)}, u32[]{:S(2)}) collective-permute-start(bf16[64,384]{1,0:T(8,128)(2,1)S(1)} %get-tuple-element.45), channel_id=1, source_target_pairs={{0,192},{1,193},{2,194},{3,195},{4,196},{5,197},{6,198},{7,199},{8... | collective-permute-start | bytes 147464 | tf_op jit(solution)/shard_map/ppermute | solution.py:340
  46.1 0.0 copy-start.1
  46.1 0.0 copy-start.2
  46.1 0.5 shard_map.166
  46.6 1.9 %collective-permute-start.10 = (bf16[32,256]{1,0:T(8,128)(2,1)S(1)}, bf16[32,256]{1,0:T(8,128)(2,1)S(1)}, u32[]{:S(2)}, u32[]{:S(2)}) collective-permute-start(bf16[32,256]{1,0:T(8,128)(2,1)S(1)} %get-tuple-element.50), channel_id=1, source_target_pairs={{0,4},{4,8},{8,12},{12,16},{16,20},{20,24},{24,28},{28,32},{32,36}... | collective-permute-start | bytes 49160 | tf_op jit(solution)/shard_map/ppermute | solution.py:309
  48.5 5.2 %collective-permute-done.10.tail_ref = bf16[32,256]{1,0:T(8,128)(2,1)S(1)} collective-permute-done((bf16[32,256]{1,0:T(8,128)(2,1)S(1)}, bf16[32,256]{1,0:T(8,128)(2,1)S(1)}, u32[]{:S(2)}, u32[]{:S(2)}) %collective-permute-start.10) | collective-permute-done | bytes 16416 | tf_op jit(solution)/shard_map/ppermute | solution.py:309
  53.8 0.6 shard_map.167
  54.4 0.7 collective-permute-start.11
  55.1 3.3 %collective-permute-start.12 = (f32[8,64]{1,0:T(8,128)S(1)}, f32[8,64]{1,0:T(8,128)S(1)}, u32[]{:S(2)}, u32[]{:S(2)}) collective-permute-start(f32[8,64]{1,0:T(8,128)S(1)} %get-tuple-element.52.s0), channel_id=1, source_target_pairs={{0,2},{1,3},{2,0},{3,1},{4,6},{5,7},{6,4},{7,5},{8,10},{9,11},{10,... | collective-permute-start | bytes 6152 | tf_op jit(solution)/shard_map/ppermute | solution.py:51
  58.3 0.9 %collective-permute-done.11.s1 = f32[8,64]{1,0:T(8,128)S(1)} collective-permute-done((f32[8,64]{1,0:T(8,128)S(1)}, f32[8,64]{1,0:T(8,128)S(1)}, u32[]{:S(2)}, u32[]{:S(2)}) %collective-permute-start.11) | collective-permute-done | bytes 2080 | tf_op jit(solution)/shard_map/ppermute | solution.py:51
  59.2 1.3 %collective-permute-start.13 = (f32[8,64]{1,0:T(8,128)S(1)}, f32[8,64]{1,0:T(8,128)S(1)}, u32[]{:S(2)}, u32[]{:S(2)}) collective-permute-start(f32[8,64]{1,0:T(8,128)S(1)} %get-tuple-element.52.s0), channel_id=1, source_target_pairs={{0,3},{1,0},{2,1},{3,2},{4,7},{5,4},{6,5},{7,6},{8,11},{9,8},{10,9... | collective-permute-start | bytes 6152 | tf_op jit(solution)/shard_map/ppermute | solution.py:51
  60.5 1.6 %shard_map.169 = (bf16[256,2048]{1,0:T(8,128)(2,1)S(1)}, bf16[256,2048]{1,0:T(8,128)(2,1)S(1)}) custom-call(bf16[256,2048]{1,0:T(8,128)(2,1)} %refs_0_.3, bf16[256,2048]{1,0:T(8,128)(2,1)} %refs_1_.1), custom_call_target="tpu_custom_call" | custom-call | flops 10000000 | tf_op jit(solution)/shard_map/pallas_call | solution.py:39
  62.0 0.8 collective-permute-done.13.s3
  62.8 0.2 shard_map.168.conv
  63.1 0.6 shard_map.170
  63.7 0.3 collective-permute-start.14
  64.0 3.9 %collective-permute-start.15 = (bf16[64,1024]{1,0:T(8,128)(2,1)S(1)}, bf16[64,1024]{1,0:T(8,128)(2,1)S(1)}, u32[]{:S(2)}, u32[]{:S(2)}) collective-permute-start(bf16[64,1024]{1,0:T(8,128)(2,1)S(1)} %get-tuple-element.57), channel_id=1, source_target_pairs={{0,2},{1,3},{2,0},{3,1},{4,6},{5,7},{6,4},{7,5},{8,10},{9,11},{10,... | collective-permute-start | bytes 393224 | tf_op jit(solution)/shard_map/ppermute | solution.py:51
  67.9 2.5 %shard_map.171 = (f32[64,512]{1,0:T(8,128)S(1)}, f32[64,512]{1,0:T(8,128)S(1)}) custom-call(bf16[64,2048]{1,0:T(8,128)(2,1)S(1)} %get-tuple-element.46.normed_ref, bf16[2048,512]{1,0:T(8,128)(2,1)} %wa.1, bf16[2048,512]{1,0:T(8,128)(2,1)} %wc.1), custom_call_target="tpu_custom_call" | custom-call | flops 268435456 | tf_op jit(solution)/shard_map/pallas_call | solution.py:39
  70.4 1.9 %collective-permute-done.15.p2 = bf16[64,1024]{1,0:T(8,128)(2,1)S(1)} collective-permute-done((bf16[64,1024]{1,0:T(8,128)(2,1)S(1)}, bf16[64,1024]{1,0:T(8,128)(2,1)S(1)}, u32[]{:S(2)}, u32[]{:S(2)}) %collective-permute-start.15) | collective-permute-done | bytes 131104 | tf_op jit(solution)/shard_map/ppermute | solution.py:51
  72.3 0.6 collective-permute-done.16.p3
  72.9 0.2 shard_map.172
  73.1 0.2 collective-permute-start.17
  73.3 3.6 %collective-permute-start.18 = (f32[8,64]{1,0:T(8,128)S(1)}, f32[8,64]{1,0:T(8,128)S(1)}, u32[]{:S(2)}, u32[]{:S(2)}) collective-permute-start(f32[8,64]{1,0:T(8,128)S(1)} %get-tuple-element.62.s0), channel_id=1, source_target_pairs={{0,2},{1,3},{2,0},{3,1},{4,6},{5,7},{6,4},{7,5},{8,10},{9,11},{10,... | collective-permute-start | bytes 6152 | tf_op jit(solution)/shard_map/ppermute | solution.py:51
  76.8 0.4 collective-permute-start.19
  77.2 0.7 collective-permute-done.17.s1
  77.9 0.5 collective-permute-done.18.s2
  78.4 2.0 %collective-permute-done.19.s3 = f32[8,64]{1,0:T(8,128)S(1)} collective-permute-done((f32[8,64]{1,0:T(8,128)S(1)}, f32[8,64]{1,0:T(8,128)S(1)}, u32[]{:S(2)}, u32[]{:S(2)}) %collective-permute-start.19) | collective-permute-done | bytes 2080 | tf_op jit(solution)/shard_map/ppermute | solution.py:51
  80.4 0.8 shard_map.173
  (16 shorter events, 0.0 us)
Async XLA Ops:
  0.0 8.6 %collective-permute-start = (bf16[16,2048]{1,0:T(8,128)(2,1)}, bf16[16,2048]{1,0:T(8,128)(2,1)S(1)}, u32[]{:S(2)}, u32[]{:S(2)}) collective-permute-start(bf16[16,2048]{1,0:T(8,128)(2,1)} %refs_0_.2), channel_id=1, source_target_pairs={{0,1},{1,2},{2,3},{3,0},{4,5},{5,6},{6,7},{7,4},{8,9},{9,10},{10,1... | collective-permute-start | bytes 196616 | tf_op jit(solution)/shard_map/ppermute | solution.py:51
  1.6 7.0 %collective-permute-start.1 = (bf16[16,2048]{1,0:T(8,128)(2,1)}, bf16[16,2048]{1,0:T(8,128)(2,1)S(1)}, u32[]{:S(2)}, u32[]{:S(2)}) collective-permute-start(bf16[16,2048]{1,0:T(8,128)(2,1)} %refs_0_.2), channel_id=1, source_target_pairs={{0,2},{1,3},{2,0},{3,1},{4,6},{5,7},{6,4},{7,5},{8,10},{9,11},{10,... | collective-permute-start | bytes 196616 | tf_op jit(solution)/shard_map/ppermute | solution.py:51
  4.5 4.5 %collective-permute-start.2 = (bf16[16,2048]{1,0:T(8,128)(2,1)}, bf16[16,2048]{1,0:T(8,128)(2,1)S(1)}, u32[]{:S(2)}, u32[]{:S(2)}) collective-permute-start(bf16[16,2048]{1,0:T(8,128)(2,1)} %refs_0_.2), channel_id=1, source_target_pairs={{0,3},{1,0},{2,1},{3,2},{4,7},{5,4},{6,5},{7,6},{8,11},{9,8},{10,9... | collective-permute-start | bytes 196616 | tf_op jit(solution)/shard_map/ppermute | solution.py:51
  9.0 28.7 %copy-start.3 = (f32[2]{0:T(128)S(1)}, f32[2]{0:T(128)}, u32[]{:S(2)}) copy-start(f32[2]{0:T(128)} %offset.1) | copy-start | bytes 28
  9.8 44.0 %copy-start.4 = (f32[31,256]{1,0:T(8,128)S(1)}, f32[31,256]{1,0:T(8,128)}, u32[]{:S(2)}) copy-start(f32[31,256]{1,0:T(8,128)} %taps.1) | copy-start | bytes 95236
  9.8 44.0 %copy-start.5 = (f32[256]{0:T(256)S(1)}, f32[256]{0:T(256)}, u32[]{:S(2)}) copy-start(f32[256]{0:T(256)} %param.28) | copy-start | bytes 3076
  22.9 14.7 %collective-permute-start.6 = (bf16[8,64,512]{2,1,0:T(8,128)(2,1)S(1)}, bf16[8,64,512]{2,1,0:T(8,128)(2,1)S(1)}, u32[]{:S(2)}, u32[]{:S(2)}) collective-permute-start(bf16[8,64,512]{2,1,0:T(8,128)(2,1)S(1)} %all_to_all.5.mine), channel_id=1, source_target_pairs={{0,4},{4,0},{1,5},{5,1},{2,6},{6,2},{3,7},{7,3},{8,12},{12,8},{9,1... | collective-permute-start | bytes 1572872 | tf_op jit(solution)/shard_map/ppermute | solution.py:333
  22.9 7.2 %collective-permute-start.3 = (bf16[64,256]{1,0:T(8,128)(2,1)S(1)}, bf16[64,256]{1,0:T(8,128)(2,1)S(1)}, u32[]{:S(2)}, u32[]{:S(2)}) collective-permute-start(bf16[64,256]{1,0:T(8,128)(2,1)S(1)} %get-tuple-element.39.q0), channel_id=1, source_target_pairs={{64,0},{128,64},{192,128},{65,1},{129,65},{193,129},{66,2},{130,66... | collective-permute-start | bytes 98312 | tf_op jit(solution)/shard_map/ppermute | solution.py:305
  24.2 10.6 %collective-permute-start.4 = (bf16[64,256]{1,0:T(8,128)(2,1)S(1)}, bf16[64,256]{1,0:T(8,128)(2,1)S(1)}, u32[]{:S(2)}, u32[]{:S(2)}) collective-permute-start(bf16[64,256]{1,0:T(8,128)(2,1)S(1)} %get-tuple-element.39.q0), channel_id=1, source_target_pairs={{128,0},{192,64},{129,1},{193,65},{130,2},{194,66},{131,3},{195,67... | collective-permute-start | bytes 98312 | tf_op jit(solution)/shard_map/ppermute | solution.py:305
  25.5 12.1 %collective-permute-start.5 = (bf16[64,256]{1,0:T(8,128)(2,1)S(1)}, bf16[64,256]{1,0:T(8,128)(2,1)S(1)}, u32[]{:S(2)}, u32[]{:S(2)}) collective-permute-start(bf16[64,256]{1,0:T(8,128)(2,1)S(1)} %get-tuple-element.39.q0), channel_id=1, source_target_pairs={{192,0},{193,1},{194,2},{195,3},{196,4},{197,5},{198,6},{199,7},{2... | collective-permute-start | bytes 98312 | tf_op jit(solution)/shard_map/ppermute | solution.py:305
  40.7 22.4 %collective-permute-start.7 = (bf16[64,384]{1,0:T(8,128)(2,1)S(1)}, bf16[64,384]{1,0:T(8,128)(2,1)S(1)}, u32[]{:S(2)}, u32[]{:S(2)}) collective-permute-start(bf16[64,384]{1,0:T(8,128)(2,1)S(1)} %get-tuple-element.43), channel_id=1, source_target_pairs={{0,64},{64,128},{128,192},{1,65},{65,129},{129,193},{2,66},{66,130... | collective-permute-start | bytes 147464 | tf_op jit(solution)/shard_map/ppermute | solution.py:340
  42.6 20.4 %collective-permute-start.8 = (bf16[64,384]{1,0:T(8,128)(2,1)S(1)}, bf16[64,384]{1,0:T(8,128)(2,1)S(1)}, u32[]{:S(2)}, u32[]{:S(2)}) collective-permute-start(bf16[64,384]{1,0:T(8,128)(2,1)S(1)} %get-tuple-element.44), channel_id=1, source_target_pairs={{0,128},{64,192},{1,129},{65,193},{2,130},{66,194},{3,131},{67,195... | collective-permute-start | bytes 147464 | tf_op jit(solution)/shard_map/ppermute | solution.py:340
  44.8 18.2 %collective-permute-start.9 = (bf16[64,384]{1,0:T(8,128)(2,1)S(1)}, bf16[64,384]{1,0:T(8,128)(2,1)S(1)}, u32[]{:S(2)}, u32[]{:S(2)}) collective-permute-start(bf16[64,384]{1,0:T(8,128)(2,1)S(1)} %get-tuple-element.45), channel_id=1, source_target_pairs={{0,192},{1,193},{2,194},{3,195},{4,196},{5,197},{6,198},{7,199},{8... | collective-permute-start | bytes 147464 | tf_op jit(solution)/shard_map/ppermute | solution.py:340
  46.1 16.7 %copy-start.1 = (f32[256]{0:T(256)S(1)}, f32[256]{0:T(256)}, u32[]{:S(2)}) copy-start(f32[256]{0:T(256)} %param.29) | copy-start | bytes 3076
  46.1 16.7 %copy-start.2 = (f32[256]{0:T(256)S(1)}, f32[256]{0:T(256)}, u32[]{:S(2)}) copy-start(f32[256]{0:T(256)} %param.30) | copy-start | bytes 3076
  46.6 7.2 %collective-permute-start.10 = (bf16[32,256]{1,0:T(8,128)(2,1)S(1)}, bf16[32,256]{1,0:T(8,128)(2,1)S(1)}, u32[]{:S(2)}, u32[]{:S(2)}) collective-permute-start(bf16[32,256]{1,0:T(8,128)(2,1)S(1)} %get-tuple-element.50), channel_id=1, source_target_pairs={{0,4},{4,8},{8,12},{12,16},{16,20},{20,24},{24,28},{28,32},{32,36}... | collective-permute-start | bytes 49160 | tf_op jit(solution)/shard_map/ppermute | solution.py:309
  54.4 4.8 %collective-permute-start.11 = (f32[8,64]{1,0:T(8,128)S(1)}, f32[8,64]{1,0:T(8,128)S(1)}, u32[]{:S(2)}, u32[]{:S(2)}) collective-permute-start(f32[8,64]{1,0:T(8,128)S(1)} %get-tuple-element.52.s0), channel_id=1, source_target_pairs={{0,1},{1,2},{2,3},{3,0},{4,5},{5,6},{6,7},{7,4},{8,9},{9,10},{10,1... | collective-permute-start | bytes 6152 | tf_op jit(solution)/shard_map/ppermute | solution.py:51
  55.1 7.0 %collective-permute-start.12 = (f32[8,64]{1,0:T(8,128)S(1)}, f32[8,64]{1,0:T(8,128)S(1)}, u32[]{:S(2)}, u32[]{:S(2)}) collective-permute-start(f32[8,64]{1,0:T(8,128)S(1)} %get-tuple-element.52.s0), channel_id=1, source_target_pairs={{0,2},{1,3},{2,0},{3,1},{4,6},{5,7},{6,4},{7,5},{8,10},{9,11},{10,... | collective-permute-start | bytes 6152 | tf_op jit(solution)/shard_map/ppermute | solution.py:51
  59.2 3.6 %collective-permute-start.13 = (f32[8,64]{1,0:T(8,128)S(1)}, f32[8,64]{1,0:T(8,128)S(1)}, u32[]{:S(2)}, u32[]{:S(2)}) collective-permute-start(f32[8,64]{1,0:T(8,128)S(1)} %get-tuple-element.52.s0), channel_id=1, source_target_pairs={{0,3},{1,0},{2,1},{3,2},{4,7},{5,4},{6,5},{7,6},{8,11},{9,8},{10,9... | collective-permute-start | bytes 6152 | tf_op jit(solution)/shard_map/ppermute | solution.py:51
  63.7 6.7 %collective-permute-start.14 = (bf16[64,1024]{1,0:T(8,128)(2,1)S(1)}, bf16[64,1024]{1,0:T(8,128)(2,1)S(1)}, u32[]{:S(2)}, u32[]{:S(2)}) collective-permute-start(bf16[64,1024]{1,0:T(8,128)(2,1)S(1)} %get-tuple-element.56), channel_id=1, source_target_pairs={{0,1},{1,2},{2,3},{3,0},{4,5},{5,6},{6,7},{7,4},{8,9},{9,10},{10,1... | collective-permute-start | bytes 393224 | tf_op jit(solution)/shard_map/ppermute | solution.py:51
  64.0 8.3 %collective-permute-start.15 = (bf16[64,1024]{1,0:T(8,128)(2,1)S(1)}, bf16[64,1024]{1,0:T(8,128)(2,1)S(1)}, u32[]{:S(2)}, u32[]{:S(2)}) collective-permute-start(bf16[64,1024]{1,0:T(8,128)(2,1)S(1)} %get-tuple-element.57), channel_id=1, source_target_pairs={{0,2},{1,3},{2,0},{3,1},{4,6},{5,7},{6,4},{7,5},{8,10},{9,11},{10,... | collective-permute-start | bytes 393224 | tf_op jit(solution)/shard_map/ppermute | solution.py:51
  67.9 12.6 %copy-start = (f32[512]{0:T(512)S(1)}, f32[512]{0:T(512)}, u32[]{:S(2)}) copy-start(f32[512]{0:T(512)} %param.33) | copy-start | bytes 6148
  67.9 5.0 %collective-permute-start.16 = (bf16[64,1024]{1,0:T(8,128)(2,1)S(1)}, bf16[64,1024]{1,0:T(8,128)(2,1)S(1)}, u32[]{:S(2)}, u32[]{:S(2)}) collective-permute-start(bf16[64,1024]{1,0:T(8,128)(2,1)S(1)} %get-tuple-element.58), channel_id=1, source_target_pairs={{0,3},{1,0},{2,1},{3,2},{4,7},{5,4},{6,5},{7,6},{8,11},{9,8},{10,9... | collective-permute-start | bytes 393224 | tf_op jit(solution)/shard_map/ppermute | solution.py:51
  73.1 4.8 %collective-permute-start.17 = (f32[8,64]{1,0:T(8,128)S(1)}, f32[8,64]{1,0:T(8,128)S(1)}, u32[]{:S(2)}, u32[]{:S(2)}) collective-permute-start(f32[8,64]{1,0:T(8,128)S(1)} %get-tuple-element.62.s0), channel_id=1, source_target_pairs={{0,1},{1,2},{2,3},{3,0},{4,5},{5,6},{6,7},{7,4},{8,9},{9,10},{10,1... | collective-permute-start | bytes 6152 | tf_op jit(solution)/shard_map/ppermute | solution.py:51
  73.3 5.2 %collective-permute-start.18 = (f32[8,64]{1,0:T(8,128)S(1)}, f32[8,64]{1,0:T(8,128)S(1)}, u32[]{:S(2)}, u32[]{:S(2)}) collective-permute-start(f32[8,64]{1,0:T(8,128)S(1)} %get-tuple-element.62.s0), channel_id=1, source_target_pairs={{0,2},{1,3},{2,0},{3,1},{4,6},{5,7},{6,4},{7,5},{8,10},{9,11},{10,... | collective-permute-start | bytes 6152 | tf_op jit(solution)/shard_map/ppermute | solution.py:51
  76.8 3.6 %collective-permute-start.19 = (f32[8,64]{1,0:T(8,128)S(1)}, f32[8,64]{1,0:T(8,128)S(1)}, u32[]{:S(2)}, u32[]{:S(2)}) collective-permute-start(f32[8,64]{1,0:T(8,128)S(1)} %get-tuple-element.62.s0), channel_id=1, source_target_pairs={{0,3},{1,0},{2,1},{3,2},{4,7},{5,4},{6,5},{7,6},{8,11},{9,8},{10,9... | collective-permute-start | bytes 6152 | tf_op jit(solution)/shard_map/ppermute | solution.py:51
where the time goes:
time: 81.6 us; the launch traced here: 81.2 us
  starting transfers between devices  30.6 us (38%)
  waiting for transfers between devices  23.8 us (29%)
  Pallas kernels  13.5 us (17%)
  blocking collectives  13.1 us (16%)
    ppermute x12, starting transfers between devices, to_rotated(): lax.ppermute(piece, 'tp', [(i, (i + d) % N_TP) for i in range(N_TP)])  19.4 us
    pallas_call x11, Pallas kernels, pallas_call(): pl.pallas_call(body, out_shape=[out_space(shape, dtype) for shape, dtype...  13.5 us
    all_to_all x1, blocking collectives, on_device(): kv_mine = lax.all_to_all(kv, ('zl', 'x'), 0, 0)  13.1 us
    ppermute x3, waiting for transfers between devices, on_device(): lax.ppermute(q, 'zh', [(i, i - d) for i in range(d, N_ZH)])  10.8 us
    ppermute x12, waiting for transfers between devices, to_rotated(): lax.ppermute(piece, 'tp', [(i, (i + d) % N_TP) for i in range(N_TP)])  7.68 us
    ppermute x3, starting transfers between devices, on_device(): lax.ppermute(m, 'zh', [(i, i + d) for i in range(N_ZH - d)])  5.42 us
    ppermute x1, waiting for transfers between devices, on_device(): lax.ppermute(tail, SP, [(i, i + 1) for i in range(lax.axis_size(SP) - 1)])  5.24 us
    ppermute x3, starting transfers between devices, on_device(): lax.ppermute(q, 'zh', [(i, i - d) for i in range(d, N_ZH)])  3.87 us
  transfers between devices with their start and end apart: 20, of which 12 were waited for; matrix products, arithmetic and copies ran while one was open for 0% of the time, Pallas kernels for 10%

commit v1 on v0

--- a/solution.py
+++ b/solution.py
@@ -51,11 +51,9 @@
     return [lax.ppermute(piece, "tp", [(i, (i + d) % N_TP) for i in range(N_TP)]) for d, piece in enumerate(pieces, 1)]
 
 
-def load_body(*refs):
-    count = (len(refs) - 1) // 2
-    sems = refs[-1]
+def started(pairs, sems):
     copies = []
-    for source, target in zip(refs[:count], refs[count:-1]):
+    for source, target in pairs:
         parts = LOAD_PARTS if source.shape[0] >= 256 else 1
         rows = source.shape[0] // parts
         for i in range(parts):
@@ -63,16 +61,24 @@
             copies.append(pltpu.make_async_copy(source.at[part], target.at[part], sems.at[len(copies)]))
     for copy in copies:
         copy.start()
-    for copy in copies:
+    return copies
+
+
+def load_body(*refs):
+    count = (len(refs) - 1) // 2
+    for copy in started(zip(refs[:count], refs[count:-1]), refs[-1]):
         copy.wait()
 
 
+def in_hbm(x):
+    return ("hbm", pltpu.with_memory_space_constraint(x, pltpu.HBM))
+
+
 def loaded(arrays):
-    arrays = [pltpu.with_memory_space_constraint(x, pltpu.HBM) for x in arrays]
     return call(
         load_body,
         [(x.shape, x.dtype) for x in arrays],
-        [("hbm", x) for x in arrays],
+        [in_hbm(x) for x in arrays],
         scratch=[pltpu.SemaphoreType.DMA((LOAD_PARTS * len(arrays),))],
         flops=10000000,
         out_space=pltpu.VMEM,
@@ -126,7 +132,9 @@
 
 def conv_body(gated_ref, tail_ref, taps, bias, conv_out, stat_out, padded):
     rows = gated_ref.shape[0]
-    padded[0:HALO, :] = tail_ref[...].astype(F32)
+    tail = tail_ref[...].astype(F32)
+    place = ((lax.axis_index("zh") * 2 + lax.axis_index("zl")) * 4 + lax.axis_index("x")) * 2 + lax.axis_index("c")
+    padded[0:HALO, :] = jnp.where(place == 0, jnp.zeros_like(tail), tail)
     padded[HALO : HALO + rows, :] = gated_ref[...].astype(F32)
     total = jnp.broadcast_to(bias[...], (rows, bias.shape[1]))
     first = HALO - (WIDTH - 1)
@@ -156,7 +164,10 @@
     normed_out[...] = (scaled * jax.nn.sigmoid(scaled)).astype(BF16)
 
 
-def attend_body(offset, q0, q1, q2, q3, mine, other, acc_out, rest_out, m1, m2, m3):
+def attend_body(
+    offset, q0, q1, q2, q3, mine, other, wa, wc, acc_out, rest_out, m1, m2, m3, wa_out, wc_out, sems
+):
+    copies = started(((wa, wa_out), (wc, wc_out)), sems)
     group = lax.axis_index("zh")
     visitors = ((q1, m1), (q2, m2), (q3, m3))
     for condition, count in ((group < N_ZH - 2, 3), (group == N_ZH - 2, 1), (group == N_ZH - 1, 0)):
@@ -164,6 +175,9 @@
         @pl.when(condition)
         def _():
             attend(offset, q0, visitors[:count], mine, other, acc_out, rest_out)
+
+    for copy in copies:
+        copy.wait()
 
 
 def attend(offset, q0, visitors, mine, other, acc_out, rest_out):
@@ -216,27 +230,32 @@
         acc = dot(jnp.concatenate(sticks, axis=1), vals)
         acc_out[:, lanes] = acc[:rows]
         rest_out[:, lanes] = rest[:rows]
-        lane = lax.broadcasted_iota(jnp.int32, (rows, 64), 1)
         for d, (_, ref) in enumerate(visitors, 1):
             part = slice(d * rows, d * rows + rows)
-            ref[:, lanes] = acc[part].astype(BF16)
-            total = rest[part][:, 0:64]
-            t1 = total.astype(BF16).astype(F32)
-            t2 = (total - t1).astype(BF16).astype(F32)
-            t3 = total - t1 - t2
-            ref[:, 256 + h * 64 : 320 + h * 64] = jnp.where(lane == 0, t1, jnp.where(lane == 1, t2, t3)).astype(BF16)
+            ref[0:rows, lanes] = acc[part].astype(BF16)
+            total = jnp.transpose(rest[part])[0:8, :]
+            high = total.astype(BF16)
+            ref[rows : rows + 8, h * 64 : h * 64 + 64] = high
+            ref[rows : rows + 8, 128 + h * 64 : 192 + h * 64] = (total - high.astype(F32)).astype(BF16)
 
 
 def merge_body(acc_ref, rest_ref, m1, m2, m3, conv, w_attn, w_conv, own_out, p1, p2, p3):
+    rows = acc_ref.shape[0]
+    messages = (m1, m2, m3)
+    group = lax.axis_index("zh")
+    held = [jnp.where(group >= d, ref[...].astype(F32), 0.0) for d, ref in enumerate(messages, 1)]
+    sent = [x[rows : rows + 8, :] for x in held]
+    totals = [x[:, h * 64 : h * 64 + 64] + x[:, 128 + h * 64 : 192 + h * 64] for x in sent for h in range(2)]
+    totals = jnp.transpose(jnp.concatenate(totals, axis=0))
     heads = []
     for h in range(2):
         lanes = slice(h * 128, h * 128 + 128)
         outside = rest_ref[:, lanes]
         total = acc_ref[:, lanes]
-        for ref in (m1, m2, m3):
-            total = total + jnp.exp2(-outside) * ref[:, lanes].astype(F32)
-            sent = ref[:, 256 + h * 64 : 320 + h * 64].astype(F32)
-            outside = outside + (sent[:, 0:1] + sent[:, 1:2] + sent[:, 2:3])
+        for d, x in enumerate(held):
+            total = total + jnp.exp2(-outside) * x[0:rows, lanes]
+            column = 8 * (2 * d + h)
+            outside = outside + totals[:, column : column + 1]
         heads.append(total.astype(BF16))
     attended = jnp.concatenate(heads, axis=1)
     convolved = conv[...]
@@ -293,7 +312,6 @@
     hidden, gain, wq, wk, wv, wga, wgb = loaded(
         (hidden_in, pre_gain.reshape(1, D), w_query, w_key, w_value, w_glu_a, w_glu_b)
     )
-    wao, wco = loaded((w_attn_out, w_conv_out))
     kv, q, normed = call(
         qkv_body,
         [((8, rows, 512), BF16), ((rows, 256), BF16), ((rows, D), BF16)],
@@ -306,11 +324,12 @@
     gated, tail = call(
         glu_body, [((rows, 256), BF16), ((HALO, 256), BF16)], [v(normed), v(wga), v(wgb)], flops=2 * rows * D * 512
     )
-    before = lax.ppermute(tail, SP, [(i, i + 1) for i in range(lax.axis_size(SP) - 1)])
+    count = lax.axis_size(SP)
+    before = lax.ppermute(tail, SP, [(i, (i + 1) % count) for i in range(count)])
     gate_a, gate_c = call(
         gates_body,
         [((rows, 512), F32), ((rows, 512), F32)],
-        [v(normed)] + [("hbm", pltpu.with_memory_space_constraint(w, pltpu.HBM)) for w in (w_gate_attn, w_gate_conv)],
+        [v(normed)] + [in_hbm(w) for w in (w_gate_attn, w_gate_conv)],
         scratch=[pltpu.VMEM((2, D, 512), BF16), pltpu.SemaphoreType.DMA((2 * LOAD_PARTS,))],
         flops=2 * rows * D * 1024,
     )
@@ -331,13 +350,18 @@
         flops=2 * rows * 256 * 100,
     )
     kv_other = lax.ppermute(kv_mine, "c", [(0, 1), (1, 0)])
-    acc, rest, *messages = call(
+    acc, rest, *messages, wao, wco = call(
         attend_body,
-        [((rows, 256), F32), ((rows, 256), F32)] + [((rows, 384), BF16)] * 3,
-        [("smem", stick_offset), v(q)] + [v(x) for x in visitors] + [v(kv_mine), v(kv_other)],
+        [((rows, 256), F32), ((rows, 256), F32)] + [((rows + 8, 256), BF16)] * 3 + [((256, D), BF16)] * 2,
+        [("smem", stick_offset), v(q)]
+        + [v(x) for x in visitors]
+        + [v(kv_mine), v(kv_other)]
+        + [in_hbm(w) for w in (w_attn_out, w_conv_out)],
+        scratch=[pltpu.SemaphoreType.DMA((2 * LOAD_PARTS,))],
         flops=2 * 2 * 256 * 1024 * 128 * 2,
-    )
-    returned = [lax.ppermute(m, "zh", [(i, i + d) for i in range(N_ZH - d)]) for d, m in enumerate(messages, 1)]
+        out_space=pltpu.VMEM,
+    )
+    returned = [lax.ppermute(m, "zh", [(i, (i + d) % N_ZH) for i in range(N_ZH)]) for d, m in enumerate(messages, 1)]
     partial = call(
         merge_body,
         [((rows, 1024), F32)] + [((rows, 1024), BF16)] * 3,

time: 81.6 us -> 80.6 us (0.988)
  the two profiles are of different devices: /device:TPU:32 before, /device:TPU:16 now
where the time goes in v1:
time: 80.6 us; the launch traced here: 80.4 us
  starting transfers between devices  34.9 us (43%)
  waiting for transfers between devices  19.2 us (24%)
  blocking collectives  14 us (17%)
  Pallas kernels  12.1 us (15%)
    ppermute x12, starting transfers between devices, to_rotated(): lax.ppermute(piece, 'tp', [(i, (i + d) % N_TP) for i in range(N_TP)])  22.2 us
    all_to_all x1, blocking collectives, on_device(): kv_mine = lax.all_to_all(kv, ('zl', 'x'), 0, 0)  14 us
    pallas_call x10, Pallas kernels, pallas_call(): pl.pallas_call(body, out_shape=[out_space(shape, dtype) for shape, dtype...  12.1 us
    ppermute x3, starting transfers between devices, on_device(): lax.ppermute(m, 'zh', [(i, (i + d) % N_ZH) for i in range(N_ZH)])  8.56 us
    ppermute x3, waiting for transfers between devices, on_device(): lax.ppermute(q, 'zh', [(i, i - d) for i in range(d, N_ZH)])  7.12 us
    ppermute x1, waiting for transfers between devices, on_device(): lax.ppermute(tail, SP, [(i, (i + 1) % count) for i in range(count)])  6.47 us
    ppermute x12, waiting for transfers between devices, to_rotated(): lax.ppermute(piece, 'tp', [(i, (i + d) % N_TP) for i in range(N_TP)])  5.58 us
    ppermute x3, starting transfers between devices, on_device(): lax.ppermute(q, 'zh', [(i, i - d) for i in range(d, N_ZH)])  4.01 us
  transfers between devices with their start and end apart: 20, of which 8 were waited for; matrix products, arithmetic and copies ran while one was open for 0% of the time, Pallas kernels for 8%

profile of v1, /device:TPU:16, one launch (start us, length us, event | category | flops | bytes accessed | tf_op | source)
XLA Modules:
  0.0 80.4 jit_solution(16251792467844361268)
XLA Ops:
  0.0 1.3 %collective-permute-start = (bf16[16,2048]{1,0:T(8,128)(2,1)}, bf16[16,2048]{1,0:T(8,128)(2,1)S(1)}, u32[]{:S(2)}, u32[]{:S(2)}) collective-permute-start(bf16[16,2048]{1,0:T(8,128)(2,1)} %refs_0_.1), channel_id=1, source_target_pairs={{0,1},{1,2},{2,3},{3,0},{4,5},{5,6},{6,7},{7,4},{8,9},{9,10},{10,1... | collective-permute-start | bytes 196616 | tf_op jit(solution)/shard_map/ppermute | solution.py:51
  1.3 0.7 collective-permute-start.2
  2.0 3.3 %collective-permute-start.1 = (bf16[16,2048]{1,0:T(8,128)(2,1)}, bf16[16,2048]{1,0:T(8,128)(2,1)S(1)}, u32[]{:S(2)}, u32[]{:S(2)}) collective-permute-start(bf16[16,2048]{1,0:T(8,128)(2,1)} %refs_0_.1), channel_id=1, source_target_pairs={{0,2},{1,3},{2,0},{3,1},{4,6},{5,7},{6,4},{7,5},{8,10},{9,11},{10,... | collective-permute-start | bytes 196616 | tf_op jit(solution)/shard_map/ppermute | solution.py:51
  5.3 2.7 %shard_map.163 = (bf16[16,2048]{1,0:T(8,128)(2,1)S(1)}, f32[1,2048]{1,0:T(1,128)S(1)}, bf16[2048,256]{1,0:T(8,128)(2,1)S(1)}, bf16[2048,256]{1,0:T(8,128)(2,1)S(...) custom-call(bf16[16,2048]{1,0:T(8,128)(2,1)} %refs_0_.1, ...), custom_call_target="tpu_custom_call" | custom-call | flops 10000000 | tf_op jit(solution)/shard_map/pallas_call | solution.py:39
  8.0 0.0 collective-permute-done.x1
  8.0 0.0 collective-permute-done.2.x3
  8.1 0.0 collective-permute-done.1.x2
  8.1 0.0 copy-start.3
  8.1 0.8 shard_map.164
  8.9 14.0 %all_to_all.5.mine = bf16[8,64,512]{2,1,0:T(8,128)(2,1)S(1)} all-to-all(bf16[8,64,512]{2,1,0:T(8,128)(2,1)S(1)} %get-tuple-element.40), channel_id=1, replica_groups=mesh['zh'=4,'zl'=2,'x'=4,'c'=2,'tp'=4] {'zl','x'}, dimensions={0} | all-to-all | bytes 1048576 | tf_op jit(solution)/shard_map/all_to_all | solution.py:322
  22.9 0.0 collective-permute-start.6
  22.9 0.0 copy-start.2
  22.9 1.4 %collective-permute-start.5 = (bf16[64,256]{1,0:T(8,128)(2,1)S(1)}, bf16[64,256]{1,0:T(8,128)(2,1)S(1)}, u32[]{:S(2)}, u32[]{:S(2)}) collective-permute-start(bf16[64,256]{1,0:T(8,128)(2,1)S(1)} %get-tuple-element.39.q0), channel_id=1, source_target_pairs={{192,0},{193,1},{194,2},{195,3},{196,4},{197,5},{198,6},{199,7},{2... | collective-permute-start | bytes 98312 | tf_op jit(solution)/shard_map/ppermute | solution.py:323
  24.3 1.3 %collective-permute-start.4 = (bf16[64,256]{1,0:T(8,128)(2,1)S(1)}, bf16[64,256]{1,0:T(8,128)(2,1)S(1)}, u32[]{:S(2)}, u32[]{:S(2)}) collective-permute-start(bf16[64,256]{1,0:T(8,128)(2,1)S(1)} %get-tuple-element.39.q0), channel_id=1, source_target_pairs={{128,0},{192,64},{129,1},{193,65},{130,2},{194,66},{131,3},{195,67... | collective-permute-start | bytes 98312 | tf_op jit(solution)/shard_map/ppermute | solution.py:323
  25.6 1.3 %collective-permute-start.3 = (bf16[64,256]{1,0:T(8,128)(2,1)S(1)}, bf16[64,256]{1,0:T(8,128)(2,1)S(1)}, u32[]{:S(2)}, u32[]{:S(2)}) collective-permute-start(bf16[64,256]{1,0:T(8,128)(2,1)S(1)} %get-tuple-element.39.q0), channel_id=1, source_target_pairs={{64,0},{128,64},{192,128},{65,1},{129,65},{193,129},{66,2},{130,66... | collective-permute-start | bytes 98312 | tf_op jit(solution)/shard_map/ppermute | solution.py:323
  26.9 4.8 %collective-permute-done.5.q3 = bf16[64,256]{1,0:T(8,128)(2,1)S(1)} collective-permute-done((bf16[64,256]{1,0:T(8,128)(2,1)S(1)}, bf16[64,256]{1,0:T(8,128)(2,1)S(1)}, u32[]{:S(2)}, u32[]{:S(2)}) %collective-permute-start.5) | collective-permute-done | bytes 32800 | tf_op jit(solution)/shard_map/ppermute | solution.py:323
  31.8 2.3 %collective-permute-done.4.q2 = bf16[64,256]{1,0:T(8,128)(2,1)S(1)} collective-permute-done((bf16[64,256]{1,0:T(8,128)(2,1)S(1)}, bf16[64,256]{1,0:T(8,128)(2,1)S(1)}, u32[]{:S(2)}, u32[]{:S(2)}) %collective-permute-start.4) | collective-permute-done | bytes 32800 | tf_op jit(solution)/shard_map/ppermute | solution.py:323
  34.1 0.0 collective-permute-done.6.other
  34.1 3.1 %shard_map.165 = (f32[64,256]{1,0:T(8,128)S(1)}, f32[64,256]{1,0:T(8,128)S(1)}, bf16[72,256]{1,0:T(8,128)(2,1)S(1)}, bf16[72,256]{1,0:T(8,128)(2,1)S(1)}, bf16[7...) custom-call(f32[2]{0:T(128)S(1)} %copy-done.3, ...), custom_call_target="tpu_custom_call" | custom-call | flops 268435456 | tf_op jit(solution)/shard_map/pallas_call | solution.py:39
  37.1 3.8 %collective-permute-start.7 = (bf16[72,256]{1,0:T(8,128)(2,1)S(1)}, bf16[72,256]{1,0:T(8,128)(2,1)S(1)}, u32[]{:S(2)}, u32[]{:S(2)}) collective-permute-start(bf16[72,256]{1,0:T(8,128)(2,1)S(1)} %get-tuple-element.43), channel_id=1, source_target_pairs={{0,64},{64,128},{128,192},{192,0},{1,65},{65,129},{129,193},{193,1... | collective-permute-start | bytes 110600 | tf_op jit(solution)/shard_map/ppermute | solution.py:364
  41.0 0.7 collective-permute-start.8
  41.7 4.0 %collective-permute-start.9 = (bf16[72,256]{1,0:T(8,128)(2,1)S(1)}, bf16[72,256]{1,0:T(8,128)(2,1)S(1)}, u32[]{:S(2)}, u32[]{:S(2)}) collective-permute-start(bf16[72,256]{1,0:T(8,128)(2,1)S(1)} %get-tuple-element.45), channel_id=1, source_target_pairs={{0,192},{64,0},{128,64},{192,128},{1,193},{65,1},{129,65},{193,129... | collective-permute-start | bytes 110600 | tf_op jit(solution)/shard_map/ppermute | solution.py:364
  45.7 0.5 shard_map.166
  46.2 0.1 collective-permute-start.10
  46.3 6.5 %collective-permute-done.10.tail_ref = bf16[32,256]{1,0:T(8,128)(2,1)S(1)} collective-permute-done((bf16[32,256]{1,0:T(8,128)(2,1)S(1)}, bf16[32,256]{1,0:T(8,128)(2,1)S(1)}, u32[]{:S(2)}, u32[]{:S(2)}) %collective-permute-start.10) | collective-permute-done | bytes 16416 | tf_op jit(solution)/shard_map/ppermute | solution.py:328
  52.8 0.6 shard_map.167
  53.4 0.6 collective-permute-start.13
  54.0 2.9 %collective-permute-start.12 = (f32[8,64]{1,0:T(8,128)S(1)}, f32[8,64]{1,0:T(8,128)S(1)}, u32[]{:S(2)}, u32[]{:S(2)}) collective-permute-start(f32[8,64]{1,0:T(8,128)S(1)} %get-tuple-element.52.s0), channel_id=1, source_target_pairs={{0,2},{1,3},{2,0},{3,1},{4,6},{5,7},{6,4},{7,5},{8,10},{9,11},{10,... | collective-permute-start | bytes 6152 | tf_op jit(solution)/shard_map/ppermute | solution.py:51
  56.9 0.3 collective-permute-done.13.s3
  57.1 2.5 %collective-permute-start.11 = (f32[8,64]{1,0:T(8,128)S(1)}, f32[8,64]{1,0:T(8,128)S(1)}, u32[]{:S(2)}, u32[]{:S(2)}) collective-permute-start(f32[8,64]{1,0:T(8,128)S(1)} %get-tuple-element.52.s0), channel_id=1, source_target_pairs={{0,1},{1,2},{2,3},{3,0},{4,5},{5,6},{6,7},{7,4},{8,9},{9,10},{10,1... | collective-permute-start | bytes 6152 | tf_op jit(solution)/shard_map/ppermute | solution.py:51
  59.6 0.0 collective-permute-done.12.s2
  59.6 1.3 %collective-permute-done.11.s1 = f32[8,64]{1,0:T(8,128)S(1)} collective-permute-done((f32[8,64]{1,0:T(8,128)S(1)}, f32[8,64]{1,0:T(8,128)S(1)}, u32[]{:S(2)}, u32[]{:S(2)}) %collective-permute-start.11) | collective-permute-done | bytes 2080 | tf_op jit(solution)/shard_map/ppermute | solution.py:51
  60.9 0.2 shard_map.168.conv
  61.2 0.0 collective-permute-done.7.m1
  61.2 0.7 shard_map.169
  61.9 2.3 %collective-permute-start.14 = (bf16[64,1024]{1,0:T(8,128)(2,1)S(1)}, bf16[64,1024]{1,0:T(8,128)(2,1)S(1)}, u32[]{:S(2)}, u32[]{:S(2)}) collective-permute-start(bf16[64,1024]{1,0:T(8,128)(2,1)S(1)} %get-tuple-element.56), channel_id=1, source_target_pairs={{0,1},{1,2},{2,3},{3,0},{4,5},{5,6},{6,7},{7,4},{8,9},{9,10},{10,1... | collective-permute-start | bytes 393224 | tf_op jit(solution)/shard_map/ppermute | solution.py:51
  64.2 0.8 collective-permute-start.15
  65.0 2.5 %collective-permute-start.16 = (bf16[64,1024]{1,0:T(8,128)(2,1)S(1)}, bf16[64,1024]{1,0:T(8,128)(2,1)S(1)}, u32[]{:S(2)}, u32[]{:S(2)}) collective-permute-start(bf16[64,1024]{1,0:T(8,128)(2,1)S(1)} %get-tuple-element.58), channel_id=1, source_target_pairs={{0,3},{1,0},{2,1},{3,2},{4,7},{5,4},{6,5},{7,6},{8,11},{9,8},{10,9... | collective-permute-start | bytes 393224 | tf_op jit(solution)/shard_map/ppermute | solution.py:51
  67.5 2.5 %shard_map.170 = (f32[64,512]{1,0:T(8,128)S(1)}, f32[64,512]{1,0:T(8,128)S(1)}) custom-call(bf16[64,2048]{1,0:T(8,128)(2,1)S(1)} %get-tuple-element.46.normed_ref, bf16[2048,512]{1,0:T(8,128)(2,1)} %wa.3, bf16[2048,512]{1,0:T(8,128)(2,1)} %wc.3), custom_call_target="tpu_custom_call" | custom-call | flops 268435456 | tf_op jit(solution)/shard_map/pallas_call | solution.py:39
  70.0 0.7 collective-permute-done.15.p2
  70.7 0.0 collective-permute-done.16.p3
  70.7 0.2 shard_map.171
  70.9 1.8 %collective-permute-start.19 = (f32[8,64]{1,0:T(8,128)S(1)}, f32[8,64]{1,0:T(8,128)S(1)}, u32[]{:S(2)}, u32[]{:S(2)}) collective-permute-start(f32[8,64]{1,0:T(8,128)S(1)} %get-tuple-element.62.s0), channel_id=1, source_target_pairs={{0,3},{1,0},{2,1},{3,2},{4,7},{5,4},{6,5},{7,6},{8,11},{9,8},{10,9... | collective-permute-start | bytes 6152 | tf_op jit(solution)/shard_map/ppermute | solution.py:51
  72.7 3.2 %collective-permute-start.18 = (f32[8,64]{1,0:T(8,128)S(1)}, f32[8,64]{1,0:T(8,128)S(1)}, u32[]{:S(2)}, u32[]{:S(2)}) collective-permute-start(f32[8,64]{1,0:T(8,128)S(1)} %get-tuple-element.62.s0), channel_id=1, source_target_pairs={{0,2},{1,3},{2,0},{3,1},{4,6},{5,7},{6,4},{7,5},{8,10},{9,11},{10,... | collective-permute-start | bytes 6152 | tf_op jit(solution)/shard_map/ppermute | solution.py:51
  75.9 0.3 collective-permute-start.17
  76.2 1.6 %collective-permute-done.18.s2 = f32[8,64]{1,0:T(8,128)S(1)} collective-permute-done((f32[8,64]{1,0:T(8,128)S(1)}, f32[8,64]{1,0:T(8,128)S(1)}, u32[]{:S(2)}, u32[]{:S(2)}) %collective-permute-start.18) | collective-permute-done | bytes 2080 | tf_op jit(solution)/shard_map/ppermute | solution.py:51
  77.8 1.7 %collective-permute-done.17.s1 = f32[8,64]{1,0:T(8,128)S(1)} collective-permute-done((f32[8,64]{1,0:T(8,128)S(1)}, f32[8,64]{1,0:T(8,128)S(1)}, u32[]{:S(2)}, u32[]{:S(2)}) %collective-permute-start.17) | collective-permute-done | bytes 2080 | tf_op jit(solution)/shard_map/ppermute | solution.py:51
  79.6 0.8 shard_map.172
  (15 shorter events, 0.0 us)
Async XLA Ops:
  0.0 8.0 %collective-permute-start = (bf16[16,2048]{1,0:T(8,128)(2,1)}, bf16[16,2048]{1,0:T(8,128)(2,1)S(1)}, u32[]{:S(2)}, u32[]{:S(2)}) collective-permute-start(bf16[16,2048]{1,0:T(8,128)(2,1)} %refs_0_.1), channel_id=1, source_target_pairs={{0,1},{1,2},{2,3},{3,0},{4,5},{5,6},{6,7},{7,4},{8,9},{9,10},{10,1... | collective-permute-start | bytes 196616 | tf_op jit(solution)/shard_map/ppermute | solution.py:51
  1.3 6.8 %collective-permute-start.2 = (bf16[16,2048]{1,0:T(8,128)(2,1)}, bf16[16,2048]{1,0:T(8,128)(2,1)S(1)}, u32[]{:S(2)}, u32[]{:S(2)}) collective-permute-start(bf16[16,2048]{1,0:T(8,128)(2,1)} %refs_0_.1), channel_id=1, source_target_pairs={{0,3},{1,0},{2,1},{3,2},{4,7},{5,4},{6,5},{7,6},{8,11},{9,8},{10,9... | collective-permute-start | bytes 196616 | tf_op jit(solution)/shard_map/ppermute | solution.py:51
  2.0 6.0 %collective-permute-start.1 = (bf16[16,2048]{1,0:T(8,128)(2,1)}, bf16[16,2048]{1,0:T(8,128)(2,1)S(1)}, u32[]{:S(2)}, u32[]{:S(2)}) collective-permute-start(bf16[16,2048]{1,0:T(8,128)(2,1)} %refs_0_.1), channel_id=1, source_target_pairs={{0,2},{1,3},{2,0},{3,1},{4,6},{5,7},{6,4},{7,5},{8,10},{9,11},{10,... | collective-permute-start | bytes 196616 | tf_op jit(solution)/shard_map/ppermute | solution.py:51
  8.1 26.0 %copy-start.3 = (f32[2]{0:T(128)S(1)}, f32[2]{0:T(128)}, u32[]{:S(2)}) copy-start(f32[2]{0:T(128)} %offset.1) | copy-start | bytes 28
  22.9 11.2 %collective-permute-start.6 = (bf16[8,64,512]{2,1,0:T(8,128)(2,1)S(1)}, bf16[8,64,512]{2,1,0:T(8,128)(2,1)S(1)}, u32[]{:S(2)}, u32[]{:S(2)}) collective-permute-start(bf16[8,64,512]{2,1,0:T(8,128)(2,1)S(1)} %all_to_all.5.mine), channel_id=1, source_target_pairs={{0,4},{4,0},{1,5},{5,1},{2,6},{6,2},{3,7},{7,3},{8,12},{12,8},{9,1... | collective-permute-start | bytes 1572872 | tf_op jit(solution)/shard_map/ppermute | solution.py:352
  22.9 29.9 %copy-start.4 = (f32[31,256]{1,0:T(8,128)S(1)}, f32[31,256]{1,0:T(8,128)}, u32[]{:S(2)}) copy-start(f32[31,256]{1,0:T(8,128)} %taps.1) | copy-start | bytes 95236
  22.9 29.9 %copy-start.5 = (f32[256]{0:T(256)S(1)}, f32[256]{0:T(256)}, u32[]{:S(2)}) copy-start(f32[256]{0:T(256)} %param.28) | copy-start | bytes 3076
  22.9 38.0 %copy-start.1 = (f32[256]{0:T(256)S(1)}, f32[256]{0:T(256)}, u32[]{:S(2)}) copy-start(f32[256]{0:T(256)} %param.29) | copy-start | bytes 3076
  22.9 38.0 %copy-start.2 = (f32[256]{0:T(256)S(1)}, f32[256]{0:T(256)}, u32[]{:S(2)}) copy-start(f32[256]{0:T(256)} %param.30) | copy-start | bytes 3076
  22.9 8.9 %collective-permute-start.5 = (bf16[64,256]{1,0:T(8,128)(2,1)S(1)}, bf16[64,256]{1,0:T(8,128)(2,1)S(1)}, u32[]{:S(2)}, u32[]{:S(2)}) collective-permute-start(bf16[64,256]{1,0:T(8,128)(2,1)S(1)} %get-tuple-element.39.q0), channel_id=1, source_target_pairs={{192,0},{193,1},{194,2},{195,3},{196,4},{197,5},{198,6},{199,7},{2... | collective-permute-start | bytes 98312 | tf_op jit(solution)/shard_map/ppermute | solution.py:323
  24.3 9.7 %collective-permute-start.4 = (bf16[64,256]{1,0:T(8,128)(2,1)S(1)}, bf16[64,256]{1,0:T(8,128)(2,1)S(1)}, u32[]{:S(2)}, u32[]{:S(2)}) collective-permute-start(bf16[64,256]{1,0:T(8,128)(2,1)S(1)} %get-tuple-element.39.q0), channel_id=1, source_target_pairs={{128,0},{192,64},{129,1},{193,65},{130,2},{194,66},{131,3},{195,67... | collective-permute-start | bytes 98312 | tf_op jit(solution)/shard_map/ppermute | solution.py:323
  25.6 8.4 %collective-permute-start.3 = (bf16[64,256]{1,0:T(8,128)(2,1)S(1)}, bf16[64,256]{1,0:T(8,128)(2,1)S(1)}, u32[]{:S(2)}, u32[]{:S(2)}) collective-permute-start(bf16[64,256]{1,0:T(8,128)(2,1)S(1)} %get-tuple-element.39.q0), channel_id=1, source_target_pairs={{64,0},{128,64},{192,128},{65,1},{129,65},{193,129},{66,2},{130,66... | collective-permute-start | bytes 98312 | tf_op jit(solution)/shard_map/ppermute | solution.py:323
  37.1 24.0 %collective-permute-start.7 = (bf16[72,256]{1,0:T(8,128)(2,1)S(1)}, bf16[72,256]{1,0:T(8,128)(2,1)S(1)}, u32[]{:S(2)}, u32[]{:S(2)}) collective-permute-start(bf16[72,256]{1,0:T(8,128)(2,1)S(1)} %get-tuple-element.43), channel_id=1, source_target_pairs={{0,64},{64,128},{128,192},{192,0},{1,65},{65,129},{129,193},{193,1... | collective-permute-start | bytes 110600 | tf_op jit(solution)/shard_map/ppermute | solution.py:364
  41.0 20.2 %collective-permute-start.8 = (bf16[72,256]{1,0:T(8,128)(2,1)S(1)}, bf16[72,256]{1,0:T(8,128)(2,1)S(1)}, u32[]{:S(2)}, u32[]{:S(2)}) collective-permute-start(bf16[72,256]{1,0:T(8,128)(2,1)S(1)} %get-tuple-element.44), channel_id=1, source_target_pairs={{0,128},{64,192},{128,0},{192,64},{1,129},{65,193},{129,1},{193,65... | collective-permute-start | bytes 110600 | tf_op jit(solution)/shard_map/ppermute | solution.py:364
  41.7 19.5 %collective-permute-start.9 = (bf16[72,256]{1,0:T(8,128)(2,1)S(1)}, bf16[72,256]{1,0:T(8,128)(2,1)S(1)}, u32[]{:S(2)}, u32[]{:S(2)}) collective-permute-start(bf16[72,256]{1,0:T(8,128)(2,1)S(1)} %get-tuple-element.45), channel_id=1, source_target_pairs={{0,192},{64,0},{128,64},{192,128},{1,193},{65,1},{129,65},{193,129... | collective-permute-start | bytes 110600 | tf_op jit(solution)/shard_map/ppermute | solution.py:364
  46.2 6.6 %collective-permute-start.10 = (bf16[32,256]{1,0:T(8,128)(2,1)S(1)}, bf16[32,256]{1,0:T(8,128)(2,1)S(1)}, u32[]{:S(2)}, u32[]{:S(2)}) collective-permute-start(bf16[32,256]{1,0:T(8,128)(2,1)S(1)} %get-tuple-element.50), channel_id=1, source_target_pairs={{0,4},{4,8},{8,12},{12,16},{16,20},{20,24},{24,28},{28,32},{32,36}... | collective-permute-start | bytes 49160 | tf_op jit(solution)/shard_map/ppermute | solution.py:328
  53.4 3.8 %collective-permute-start.13 = (f32[8,64]{1,0:T(8,128)S(1)}, f32[8,64]{1,0:T(8,128)S(1)}, u32[]{:S(2)}, u32[]{:S(2)}) collective-permute-start(f32[8,64]{1,0:T(8,128)S(1)} %get-tuple-element.52.s0), channel_id=1, source_target_pairs={{0,3},{1,0},{2,1},{3,2},{4,7},{5,4},{6,5},{7,6},{8,11},{9,8},{10,9... | collective-permute-start | bytes 6152 | tf_op jit(solution)/shard_map/ppermute | solution.py:51
  54.0 5.7 %collective-permute-start.12 = (f32[8,64]{1,0:T(8,128)S(1)}, f32[8,64]{1,0:T(8,128)S(1)}, u32[]{:S(2)}, u32[]{:S(2)}) collective-permute-start(f32[8,64]{1,0:T(8,128)S(1)} %get-tuple-element.52.s0), channel_id=1, source_target_pairs={{0,2},{1,3},{2,0},{3,1},{4,6},{5,7},{6,4},{7,5},{8,10},{9,11},{10,... | collective-permute-start | bytes 6152 | tf_op jit(solution)/shard_map/ppermute | solution.py:51
  57.1 3.8 %collective-permute-start.11 = (f32[8,64]{1,0:T(8,128)S(1)}, f32[8,64]{1,0:T(8,128)S(1)}, u32[]{:S(2)}, u32[]{:S(2)}) collective-permute-start(f32[8,64]{1,0:T(8,128)S(1)} %get-tuple-element.52.s0), channel_id=1, source_target_pairs={{0,1},{1,2},{2,3},{3,0},{4,5},{5,6},{6,7},{7,4},{8,9},{9,10},{10,1... | collective-permute-start | bytes 6152 | tf_op jit(solution)/shard_map/ppermute | solution.py:51
  61.9 8.1 %collective-permute-start.14 = (bf16[64,1024]{1,0:T(8,128)(2,1)S(1)}, bf16[64,1024]{1,0:T(8,128)(2,1)S(1)}, u32[]{:S(2)}, u32[]{:S(2)}) collective-permute-start(bf16[64,1024]{1,0:T(8,128)(2,1)S(1)} %get-tuple-element.56), channel_id=1, source_target_pairs={{0,1},{1,2},{2,3},{3,0},{4,5},{5,6},{6,7},{7,4},{8,9},{9,10},{10,1... | collective-permute-start | bytes 393224 | tf_op jit(solution)/shard_map/ppermute | solution.py:51
  64.2 6.5 %collective-permute-start.15 = (bf16[64,1024]{1,0:T(8,128)(2,1)S(1)}, bf16[64,1024]{1,0:T(8,128)(2,1)S(1)}, u32[]{:S(2)}, u32[]{:S(2)}) collective-permute-start(bf16[64,1024]{1,0:T(8,128)(2,1)S(1)} %get-tuple-element.57), channel_id=1, source_target_pairs={{0,2},{1,3},{2,0},{3,1},{4,6},{5,7},{6,4},{7,5},{8,10},{9,11},{10,... | collective-permute-start | bytes 393224 | tf_op jit(solution)/shard_map/ppermute | solution.py:51
  65.0 14.6 %copy-start = (f32[512]{0:T(512)S(1)}, f32[512]{0:T(512)}, u32[]{:S(2)}) copy-start(f32[512]{0:T(512)} %param.33) | copy-start | bytes 6148
  65.0 5.7 %collective-permute-start.16 = (bf16[64,1024]{1,0:T(8,128)(2,1)S(1)}, bf16[64,1024]{1,0:T(8,128)(2,1)S(1)}, u32[]{:S(2)}, u32[]{:S(2)}) collective-permute-start(bf16[64,1024]{1,0:T(8,128)(2,1)S(1)} %get-tuple-element.58), channel_id=1, source_target_pairs={{0,3},{1,0},{2,1},{3,2},{4,7},{5,4},{6,5},{7,6},{8,11},{9,8},{10,9... | collective-permute-start | bytes 393224 | tf_op jit(solution)/shard_map/ppermute | solution.py:51
  70.9 5.3 %collective-permute-start.19 = (f32[8,64]{1,0:T(8,128)S(1)}, f32[8,64]{1,0:T(8,128)S(1)}, u32[]{:S(2)}, u32[]{:S(2)}) collective-permute-start(f32[8,64]{1,0:T(8,128)S(1)} %get-tuple-element.62.s0), channel_id=1, source_target_pairs={{0,3},{1,0},{2,1},{3,2},{4,7},{5,4},{6,5},{7,6},{8,11},{9,8},{10,9... | collective-permute-start | bytes 6152 | tf_op jit(solution)/shard_map/ppermute | solution.py:51
  72.7 5.1 %collective-permute-start.18 = (f32[8,64]{1,0:T(8,128)S(1)}, f32[8,64]{1,0:T(8,128)S(1)}, u32[]{:S(2)}, u32[]{:S(2)}) collective-permute-start(f32[8,64]{1,0:T(8,128)S(1)} %get-tuple-element.62.s0), channel_id=1, source_target_pairs={{0,2},{1,3},{2,0},{3,1},{4,6},{5,7},{6,4},{7,5},{8,10},{9,11},{10,... | collective-permute-start | bytes 6152 | tf_op jit(solution)/shard_map/ppermute | solution.py:51
  75.9 3.6 %collective-permute-start.17 = (f32[8,64]{1,0:T(8,128)S(1)}, f32[8,64]{1,0:T(8,128)S(1)}, u32[]{:S(2)}, u32[]{:S(2)}) collective-permute-start(f32[8,64]{1,0:T(8,128)S(1)} %get-tuple-element.62.s0), channel_id=1, source_target_pairs={{0,1},{1,2},{2,3},{3,0},{4,5},{5,6},{6,7},{7,4},{8,9},{9,10},{10,1... | collective-permute-start | bytes 6152 | tf_op jit(solution)/shard_map/ppermute | solution.py:51

commit v2 on v1

--- a/solution.py
+++ b/solution.py
@@ -85,7 +85,7 @@
     )
 
 
-def qkv_body(x0, x1, x2, x3, gain, wq, wk, wv, kv_out, q_out, normed_out, rows):
+def qkv_body(x0, x1, x2, x3, gain, wq, wk, wv, wa, wb, kv_out, q_out, normed_out, gated_out, tail_out, rows):
     me = lax.axis_index("tp")
     for d, ref in enumerate((x0, x1, x2, x3)):
         source = lax.rem(me + N_TP - d, N_TP)
@@ -100,10 +100,6 @@
         kv_out[i, :, 0:256] = keys
         kv_out[i, :, 256:512] = vals
     q_out[...] = dot(normed, wq[...]).astype(BF16)
-
-
-def glu_body(normed_ref, wa, wb, gated_out, tail_out):
-    normed = normed_ref[...]
     left = dot(normed, wa[...]).astype(BF16).astype(F32)
     right = dot(normed, wb[...]).astype(BF16).astype(F32)
     gated = (left * jax.nn.sigmoid(right)).astype(BF16)
@@ -111,23 +107,10 @@
     tail_out[...] = gated[gated.shape[0] - HALO :, :]
 
 
-def gates_body(normed_ref, wa, wc, ga_out, gc_out, held, sems):
-    rows = D // LOAD_PARTS
-    copies = []
-    for i in range(LOAD_PARTS):
-        part = pl.ds(i * rows, rows)
-        for j, source in enumerate((wa, wc)):
-            copies.append(pltpu.make_async_copy(source.at[part], held.at[j, part], sems.at[len(copies)]))
-    for copy in copies:
-        copy.start()
-    totals = [0.0, 0.0]
-    for i in range(LOAD_PARTS):
-        part = slice(i * rows, i * rows + rows)
-        for j in range(2):
-            copies[2 * i + j].wait()
-            totals[j] = totals[j] + dot(normed_ref[:, part], held[j, part, :])
-    ga_out[...] = jax.nn.sigmoid(totals[0].astype(BF16).astype(F32))
-    gc_out[...] = jax.nn.sigmoid(totals[1].astype(BF16).astype(F32))
+def gates_body(normed_ref, wa, wc, ga_out, gc_out):
+    normed = normed_ref[...]
+    ga_out[...] = jax.nn.sigmoid(dot(normed, wa[...]).astype(BF16).astype(F32))
+    gc_out[...] = jax.nn.sigmoid(dot(normed, wc[...]).astype(BF16).astype(F32))
 
 
 def conv_body(gated_ref, tail_ref, taps, bias, conv_out, stat_out, padded):
@@ -164,79 +147,79 @@
     normed_out[...] = (scaled * jax.nn.sigmoid(scaled)).astype(BF16)
 
 
-def attend_body(
-    offset, q0, q1, q2, q3, mine, other, wa, wc, acc_out, rest_out, m1, m2, m3, wa_out, wc_out, sems
-):
-    copies = started(((wa, wa_out), (wc, wc_out)), sems)
+def visit_body(offset, q1, q2, q3, mine, other, m1, m2, m3):
     group = lax.axis_index("zh")
-    visitors = ((q1, m1), (q2, m2), (q3, m3))
-    for condition, count in ((group < N_ZH - 2, 3), (group == N_ZH - 2, 1), (group == N_ZH - 1, 0)):
+    pairs = ((q1, m1), (q2, m2), (q3, m3))
+    rows = q1.shape[0]
+    for condition, count in ((group < N_ZH - 2, 3), (group == N_ZH - 2, 1)):
 
         @pl.when(condition)
         def _():
-            attend(offset, q0, visitors[:count], mine, other, acc_out, rest_out)
-
-    for copy in copies:
-        copy.wait()
-
-
-def attend(offset, q0, visitors, mine, other, acc_out, rest_out):
+            suffix = suffix_matrix()
+            for h in range(2):
+                acc, rest = attend(offset, h, [q for q, _ in pairs[:count]], mine, other, suffix, False)
+                for d, (_, ref) in enumerate(pairs[:count]):
+                    part = slice(d * rows, d * rows + rows)
+                    ref[0:rows, h * 128 : h * 128 + 128] = acc[part].astype(BF16)
+                    total = jnp.transpose(rest[part])[0:8, :]
+                    high = total.astype(BF16)
+                    ref[rows : rows + 8, h * 64 : h * 64 + 64] = high
+                    ref[rows : rows + 8, 128 + h * 64 : 192 + h * 64] = (total - high.astype(F32)).astype(BF16)
+
+
+def own_body(offset, q, mine, other, acc_out, rest_out):
+    suffix = suffix_matrix()
+    for h in range(2):
+        lanes = slice(h * 128, h * 128 + 128)
+        acc_out[:, lanes], rest_out[:, lanes] = attend(offset, h, [q], mine, other, suffix, True)
+
+
+def place_of(index):
+    return (index + lax.axis_index("c") * 64) & 127
+
+
+def suffix_matrix():
+    row_place = place_of(lax.broadcasted_iota(jnp.int32, (256, 256), 0))
+    column = lax.broadcasted_iota(jnp.int32, (256, 256), 1)
+    return jnp.where((column >= 128) | (row_place >= place_of(column)), 1.0, 0.0).astype(BF16)
+
+
+def attend(offset, h, query_refs, mine, other, suffix, own):
     core = lax.axis_index("c")
-    rows = q0.shape[0]
     blocks = mine.shape[0]
-    total_rows = rows * (1 + len(visitors))
+    rows = sum(q.shape[0] for q in query_refs)
+    place = place_of(lax.broadcasted_iota(jnp.int32, (1, 128), 1))
     position = (lax.axis_index("zl") * 4 + lax.axis_index("x")) * 128 + core * 64
     query_pos = position + lax.broadcasted_iota(jnp.int32, (rows, 128), 0)
-    index = lax.broadcasted_iota(jnp.int32, (1, 128), 1)
-    place = lax.rem(index + core * 64, 128)
-    row_index = lax.rem(lax.broadcasted_iota(jnp.int32, (256, 256), 0), 128)
-    col_index = lax.broadcasted_iota(jnp.int32, (256, 256), 1)
-    row_place = lax.rem(row_index + core * 64, 128)
-    col_place = lax.rem(col_index + core * 64, 128)
-    suffix = jnp.where((col_index >= 128) | (row_place >= col_place), 1.0, 0.0).astype(BF16)
-    scale = LOG2E / math.sqrt(HEAD_DIM)
-
     tiles = range(blocks)
     span = [slice(b * 128, b * 128 + 128) for b in tiles]
-    own_causal = [(b * 128 + place) < query_pos for b in tiles]
-
-    def for_own(b, x):
-        masked = jnp.where(own_causal[b], x[:rows], 0.0)
-        return jnp.concatenate([masked, x[rows:]], axis=0) if visitors else masked
-
-    for h in range(2):
-        lanes = slice(h * 128, h * 128 + 128)
-        value_lanes = slice(256 + h * 128, 256 + h * 128 + 128)
-        queries = jnp.concatenate([q[:, lanes] for q in [q0] + [q for q, _ in visitors]], axis=0)
-        keys = jnp.concatenate([ref[b, :, lanes] for b in tiles for ref in (mine, other)], axis=0)
-        vals = jnp.concatenate([ref[b, :, value_lanes] for b in tiles for ref in (mine, other)], axis=0)
-        scores = lax.dot_general(queries, keys, (((1,), (1,)), ((), ())), preferred_element_type=F32)
-        scores = scores * scale + offset[h] * LOG2E
-        soft = jnp.maximum(scores, 0.0) + jnp.log2(1.0 + jnp.exp2(-jnp.abs(scores)))
-        split = []
-        for b in tiles:
-            part = for_own(b, soft[:, span[b]])
-            high = part.astype(BF16)
-            low = (part - high.astype(F32)).astype(BF16)
-            split.append(jnp.concatenate([high, low], axis=1))
-        sums = dot(jnp.concatenate(split, axis=0), suffix)
-        sums = [sums[b * total_rows : (b + 1) * total_rows] for b in tiles]
-        rest = jnp.zeros((total_rows, 128), F32)
-        sticks = [None] * blocks
-        for b in reversed(tiles):
-            stick = for_own(b, jnp.exp2(scores[:, span[b]] - (sums[b][:, 0:128] + rest)))
-            sticks[b] = stick.astype(BF16)
-            rest = rest + sums[b][:, 128:256]
-        acc = dot(jnp.concatenate(sticks, axis=1), vals)
-        acc_out[:, lanes] = acc[:rows]
-        rest_out[:, lanes] = rest[:rows]
-        for d, (_, ref) in enumerate(visitors, 1):
-            part = slice(d * rows, d * rows + rows)
-            ref[0:rows, lanes] = acc[part].astype(BF16)
-            total = jnp.transpose(rest[part])[0:8, :]
-            high = total.astype(BF16)
-            ref[rows : rows + 8, h * 64 : h * 64 + 64] = high
-            ref[rows : rows + 8, 128 + h * 64 : 192 + h * 64] = (total - high.astype(F32)).astype(BF16)
+    lanes = slice(h * 128, h * 128 + 128)
+    value_lanes = slice(256 + h * 128, 256 + h * 128 + 128)
+
+    def causal(b, x):
+        return jnp.where((b * 128 + place) < query_pos, x, 0.0) if own else x
+
+    queries = jnp.concatenate([q[:, lanes] for q in query_refs], axis=0)
+    keys = jnp.concatenate([ref[b, :, lanes] for b in tiles for ref in (mine, other)], axis=0)
+    vals = jnp.concatenate([ref[b, :, value_lanes] for b in tiles for ref in (mine, other)], axis=0)
+    scores = lax.dot_general(queries, keys, (((1,), (1,)), ((), ())), preferred_element_type=F32)
+    scores = scores * (LOG2E / math.sqrt(HEAD_DIM)) + offset[h] * LOG2E
+    soft = jnp.maximum(scores, 0.0) + jnp.log2(1.0 + jnp.exp2(-jnp.abs(scores)))
+    split = []
+    for b in tiles:
+        part = causal(b, soft[:, span[b]])
+        high = part.astype(BF16)
+        low = (part - high.astype(F32)).astype(BF16)
+        split.append(jnp.concatenate([high, low], axis=1))
+    sums = dot(jnp.concatenate(split, axis=0), suffix)
+    sums = [sums[b * rows : (b + 1) * rows] for b in tiles]
+    rest = jnp.zeros((rows, 128), F32)
+    sticks = [None] * blocks
+    for b in reversed(tiles):
+        stick = causal(b, jnp.exp2(scores[:, span[b]] - (sums[b][:, 0:128] + rest)))
+        sticks[b] = stick.astype(BF16)
+        rest = rest + sums[b][:, 128:256]
+    return dot(jnp.concatenate(sticks, axis=1), vals), rest
 
 
 def merge_body(acc_ref, rest_ref, m1, m2, m3, conv, w_attn, w_conv, own_out, p1, p2, p3):
@@ -312,25 +295,21 @@
     hidden, gain, wq, wk, wv, wga, wgb = loaded(
         (hidden_in, pre_gain.reshape(1, D), w_query, w_key, w_value, w_glu_a, w_glu_b)
     )
-    kv, q, normed = call(
+    kv, q, normed, gated, tail = call(
         qkv_body,
-        [((8, rows, 512), BF16), ((rows, 256), BF16), ((rows, D), BF16)],
-        [v(p) for p in [hidden] + pieces] + [v(gain), v(wq), v(wk), v(wv)],
+        [((8, rows, 512), BF16), ((rows, 256), BF16), ((rows, D), BF16), ((rows, 256), BF16), ((HALO, 256), BF16)],
+        [v(p) for p in [hidden] + pieces] + [v(gain), v(wq), v(wk), v(wv), v(wga), v(wgb)],
         scratch=[pltpu.VMEM((rows, D), BF16)],
         flops=2 * rows * D * 768,
     )
     kv_mine = lax.all_to_all(kv, ("zl", "x"), 0, 0)
     visitors = [lax.ppermute(q, "zh", [(i, i - d) for i in range(d, N_ZH)]) for d in range(1, N_ZH)]
-    gated, tail = call(
-        glu_body, [((rows, 256), BF16), ((HALO, 256), BF16)], [v(normed), v(wga), v(wgb)], flops=2 * rows * D * 512
-    )
     count = lax.axis_size(SP)
     before = lax.ppermute(tail, SP, [(i, (i + 1) % count) for i in range(count)])
     gate_a, gate_c = call(
         gates_body,
         [((rows, 512), F32), ((rows, 512), F32)],
-        [v(normed)] + [in_hbm(w) for w in (w_gate_attn, w_gate_conv)],
-        scratch=[pltpu.VMEM((2, D, 512), BF16), pltpu.SemaphoreType.DMA((2 * LOAD_PARTS,))],
+        [v(normed), v(w_gate_attn), v(w_gate_conv)],
         flops=2 * rows * D * 1024,
     )
     convolved, stat = call(
@@ -350,22 +329,23 @@
         flops=2 * rows * 256 * 100,
     )
     kv_other = lax.ppermute(kv_mine, "c", [(0, 1), (1, 0)])
-    acc, rest, *messages, wao, wco = call(
-        attend_body,
-        [((rows, 256), F32), ((rows, 256), F32)] + [((rows + 8, 256), BF16)] * 3 + [((256, D), BF16)] * 2,
-        [("smem", stick_offset), v(q)]
-        + [v(x) for x in visitors]
-        + [v(kv_mine), v(kv_other)]
-        + [in_hbm(w) for w in (w_attn_out, w_conv_out)],
-        scratch=[pltpu.SemaphoreType.DMA((2 * LOAD_PARTS,))],
-        flops=2 * 2 * 256 * 1024 * 128 * 2,
-        out_space=pltpu.VMEM,
+    messages = call(
+        visit_body,
+        [((rows + 8, 256), BF16)] * 3,
+        [("smem", stick_offset)] + [v(x) for x in visitors] + [v(kv_mine), v(kv_other)],
+        flops=2 * 2 * 192 * 1024 * 128 * 2,
+    )
+    acc, rest = call(
+        own_body,
+        [((rows, 256), F32), ((rows, 256), F32)],
+        [("smem", stick_offset), v(q), v(kv_mine), v(kv_other)],
+        flops=2 * 2 * 64 * 1024 * 128 * 2,
     )
     returned = [lax.ppermute(m, "zh", [(i, (i + d) % N_ZH) for i in range(N_ZH)]) for d, m in enumerate(messages, 1)]
     partial = call(
         merge_body,
         [((rows, 1024), F32)] + [((rows, 1024), BF16)] * 3,
-        [v(acc), v(rest)] + [v(m) for m in returned] + [v(conv_normed), v(wao), v(wco)],
+        [v(acc), v(rest)] + [v(m) for m in returned] + [v(conv_normed), v(w_attn_out), v(w_conv_out)],
         flops=4 * rows * 256 * D,
     )
     pieces = [partial[0]] + to_rotated(partial[1:])

time: 80.6 us -> 81.3 us (level)
  waiting for transfers between devices: 19.2 us -> 21.5 us
  starting transfers between devices: 34.9 us -> 33.8 us
    ppermute x12, waiting for transfers between devices: 5.58 us -> 7.91 us  [to_rotated(): lax.ppermute(piece, 'tp', [(i, (i + d) % N_TP) for i in range(N_TP)])]
    ppermute x12, starting transfers between devices: 22.2 us -> 21.3 us  [to_rotated(): lax.ppermute(piece, 'tp', [(i, (i + d) % N_TP) for i in range(N_TP)])]
  transfers between devices with their start and end apart: 20 -> 20, of which waited for: 8 -> 8; matrix products, arithmetic and copies ran while one was open for 0% -> 0% of each run, Pallas kernels for 8% -> 7%
where the time goes in v2:
time: 81.3 us; the launch traced here: 81.2 us
  starting transfers between devices  33.8 us (42%)
  waiting for transfers between devices  21.5 us (26%)
  blocking collectives  14.1 us (17%)
  Pallas kernels  11.4 us (14%)
    ppermute x12, starting transfers between devices, to_rotated(): lax.ppermute(piece, 'tp', [(i, (i + d) % N_TP) for i in range(N_TP)])  21.3 us
    all_to_all x1, blocking collectives, on_device(): kv_mine = lax.all_to_all(kv, ('zl', 'x'), 0, 0)  14.1 us
    pallas_call x10, Pallas kernels, pallas_call(): pl.pallas_call(body, out_shape=[out_space(shape, dtype) for shape, dtype...  11.4 us
    ppermute x3, starting transfers between devices, on_device(): lax.ppermute(m, 'zh', [(i, (i + d) % N_ZH) for i in range(N_ZH)])  8.56 us
    ppermute x12, waiting for transfers between devices, to_rotated(): lax.ppermute(piece, 'tp', [(i, (i + d) % N_TP) for i in range(N_TP)])  7.91 us
    ppermute x3, waiting for transfers between devices, on_device(): lax.ppermute(q, 'zh', [(i, i - d) for i in range(d, N_ZH)])  7.12 us
    ppermute x1, waiting for transfers between devices, on_device(): lax.ppermute(tail, SP, [(i, (i + 1) % count) for i in range(count)])  6.48 us
    ppermute x3, starting transfers between devices, on_device(): lax.ppermute(q, 'zh', [(i, i - d) for i in range(d, N_ZH)])  3.87 us
  transfers between devices with their start and end apart: 20, of which 8 were waited for; matrix products, arithmetic and copies ran while one was open for 0% of the time, Pallas kernels for 7%

profile of v2, /device:TPU:16, one launch (start us, length us, event | category | flops | bytes accessed | tf_op | source)
XLA Modules:
  0.0 81.2 jit_solution(4200304688577968372)
XLA Ops:
  0.0 1.3 %collective-permute-start = (bf16[16,2048]{1,0:T(8,128)(2,1)}, bf16[16,2048]{1,0:T(8,128)(2,1)S(1)}, u32[]{:S(2)}, u32[]{:S(2)}) collective-permute-start(bf16[16,2048]{1,0:T(8,128)(2,1)} %refs_0_.1), channel_id=1, source_target_pairs={{0,1},{1,2},{2,3},{3,0},{4,5},{5,6},{6,7},{7,4},{8,9},{9,10},{10,1... | collective-permute-start | bytes 196616 | tf_op jit(solution)/shard_map/ppermute | solution.py:51
  1.3 0.7 collective-permute-start.2
  2.0 3.3 %collective-permute-start.1 = (bf16[16,2048]{1,0:T(8,128)(2,1)}, bf16[16,2048]{1,0:T(8,128)(2,1)S(1)}, u32[]{:S(2)}, u32[]{:S(2)}) collective-permute-start(bf16[16,2048]{1,0:T(8,128)(2,1)} %refs_0_.1), channel_id=1, source_target_pairs={{0,2},{1,3},{2,0},{3,1},{4,6},{5,7},{6,4},{7,5},{8,10},{9,11},{10,... | collective-permute-start | bytes 196616 | tf_op jit(solution)/shard_map/ppermute | solution.py:51
  5.3 2.7 %shard_map.163 = (bf16[16,2048]{1,0:T(8,128)(2,1)S(1)}, f32[1,2048]{1,0:T(1,128)S(1)}, bf16[2048,256]{1,0:T(8,128)(2,1)S(1)}, bf16[2048,256]{1,0:T(8,128)(2,1)S(...) custom-call(bf16[16,2048]{1,0:T(8,128)(2,1)} %refs_0_.1, ...), custom_call_target="tpu_custom_call" | custom-call | flops 10000000 | tf_op jit(solution)/shard_map/pallas_call | solution.py:39
  8.0 0.0 collective-permute-done.2.x3
  8.1 0.0 collective-permute-done.1.x2
  8.1 0.0 copy-start.5
  8.1 0.0 copy-start.3
  8.1 1.2 %shard_map.164 = (bf16[8,64,512]{2,1,0:T(8,128)(2,1)S(1)}, bf16[64,256]{1,0:T(8,128)(2,1)S(1)}, bf16[64,2048]{1,0:T(8,128)(2,1)S(1)}, bf16[64,256]{1,0:T(8,128)(2,1)S(1)}, bf16[32,256]{1,0:T(8,128)(2,1)S(1)}) custom-call(bf16[16,2048]{1,0:T(8,128)(2,1)S(1)} %get-tuple-element.32.x0, bf16[16,2048]{1,0:T(8,128)(2,1)S(1)} %collective-permute-done.x1, ...), custom_call_target="tpu_custom_call" | custom-call | flops 201326592 | tf_op jit(solution)/shard_map/pallas_call | solution.py:39
  9.3 0.0 copy-start.8
  9.3 0.0 copy-start.9
  9.3 0.0 copy-start.6
  9.3 0.0 copy-start.7
  9.3 0.0 copy-start.2
  9.3 14.1 %all_to_all.5.mine = bf16[8,64,512]{2,1,0:T(8,128)(2,1)S(1)} all-to-all(bf16[8,64,512]{2,1,0:T(8,128)(2,1)S(1)} %get-tuple-element.40), channel_id=1, replica_groups=mesh['zh'=4,'zl'=2,'x'=4,'c'=2,'tp'=4] {'zl','x'}, dimensions={0} | all-to-all | bytes 1048576 | tf_op jit(solution)/shard_map/all_to_all | solution.py:305
  23.5 1.3 %collective-permute-start.6 = (bf16[64,256]{1,0:T(8,128)(2,1)S(1)}, bf16[64,256]{1,0:T(8,128)(2,1)S(1)}, u32[]{:S(2)}, u32[]{:S(2)}) collective-permute-start(bf16[64,256]{1,0:T(8,128)(2,1)S(1)} %get-tuple-element.39.q), channel_id=1, source_target_pairs={{192,0},{193,1},{194,2},{195,3},{196,4},{197,5},{198,6},{199,7},{2... | collective-permute-start | bytes 98312 | tf_op jit(solution)/shard_map/ppermute | solution.py:306
  24.8 1.3 %collective-permute-start.5 = (bf16[64,256]{1,0:T(8,128)(2,1)S(1)}, bf16[64,256]{1,0:T(8,128)(2,1)S(1)}, u32[]{:S(2)}, u32[]{:S(2)}) collective-permute-start(bf16[64,256]{1,0:T(8,128)(2,1)S(1)} %get-tuple-element.39.q), channel_id=1, source_target_pairs={{128,0},{192,64},{129,1},{193,65},{130,2},{194,66},{131,3},{195,67... | collective-permute-start | bytes 98312 | tf_op jit(solution)/shard_map/ppermute | solution.py:306
  26.1 1.3 %collective-permute-start.4 = (bf16[64,256]{1,0:T(8,128)(2,1)S(1)}, bf16[64,256]{1,0:T(8,128)(2,1)S(1)}, u32[]{:S(2)}, u32[]{:S(2)}) collective-permute-start(bf16[64,256]{1,0:T(8,128)(2,1)S(1)} %get-tuple-element.39.q), channel_id=1, source_target_pairs={{64,0},{128,64},{192,128},{65,1},{129,65},{193,129},{66,2},{130,66... | collective-permute-start | bytes 98312 | tf_op jit(solution)/shard_map/ppermute | solution.py:306
  27.4 4.8 %collective-permute-done.6.q3 = bf16[64,256]{1,0:T(8,128)(2,1)S(1)} collective-permute-done((bf16[64,256]{1,0:T(8,128)(2,1)S(1)}, bf16[64,256]{1,0:T(8,128)(2,1)S(1)}, u32[]{:S(2)}, u32[]{:S(2)}) %collective-permute-start.6) | collective-permute-done | bytes 32800 | tf_op jit(solution)/shard_map/ppermute | solution.py:306
  32.2 2.3 %collective-permute-done.5.q2 = bf16[64,256]{1,0:T(8,128)(2,1)S(1)} collective-permute-done((bf16[64,256]{1,0:T(8,128)(2,1)S(1)}, bf16[64,256]{1,0:T(8,128)(2,1)S(1)}, u32[]{:S(2)}, u32[]{:S(2)}) %collective-permute-start.5) | collective-permute-done | bytes 32800 | tf_op jit(solution)/shard_map/ppermute | solution.py:306
  34.5 0.0 collective-permute-done.4.q1
  34.5 0.0 copy-start.1
  34.5 2.5 %shard_map.166 = (bf16[72,256]{1,0:T(8,128)(2,1)S(1)}, bf16[72,256]{1,0:T(8,128)(2,1)S(1)}, bf16[72,256]{1,0:T(8,128)(2,1)S(1)}) custom-call(f32[2]{0:T(128)S(1)} %copy-done.5, bf16[64,256]{1,0:T(8,128)(2,1)S(1)} %collective-permute-done.4.q1, bf16[64,256]{1,0:T(8,128)(2,1)S(1)} %collective-permute-done.5.q2, bf16[64,256]{1,0:T(8,128)(2,1)S(1)} %collective-permute-done.6.q3, ...), custom_call_target="tpu_custom_call" | custom-call | flops 201326592 | tf_op jit(solution)/shard_map/pallas_call | solution.py:39
  37.0 0.0 copy-start
  37.0 3.8 %collective-permute-start.7 = (bf16[72,256]{1,0:T(8,128)(2,1)S(1)}, bf16[72,256]{1,0:T(8,128)(2,1)S(1)}, u32[]{:S(2)}, u32[]{:S(2)}) collective-permute-start(bf16[72,256]{1,0:T(8,128)(2,1)S(1)} %get-tuple-element.43), channel_id=1, source_target_pairs={{0,64},{64,128},{128,192},{192,0},{1,65},{65,129},{129,193},{193,1... | collective-permute-start | bytes 110600 | tf_op jit(solution)/shard_map/ppermute | solution.py:344
  40.9 0.7 collective-permute-start.8
  41.6 4.0 %collective-permute-start.9 = (bf16[72,256]{1,0:T(8,128)(2,1)S(1)}, bf16[72,256]{1,0:T(8,128)(2,1)S(1)}, u32[]{:S(2)}, u32[]{:S(2)}) collective-permute-start(bf16[72,256]{1,0:T(8,128)(2,1)S(1)} %get-tuple-element.45), channel_id=1, source_target_pairs={{0,192},{64,0},{128,64},{192,128},{1,193},{65,1},{129,65},{193,129... | collective-permute-start | bytes 110600 | tf_op jit(solution)/shard_map/ppermute | solution.py:344
  45.6 6.5 %collective-permute-done.10.tail_ref = bf16[32,256]{1,0:T(8,128)(2,1)S(1)} collective-permute-done((bf16[32,256]{1,0:T(8,128)(2,1)S(1)}, bf16[32,256]{1,0:T(8,128)(2,1)S(1)}, u32[]{:S(2)}, u32[]{:S(2)}) %collective-permute-start.10) | collective-permute-done | bytes 16416 | tf_op jit(solution)/shard_map/ppermute | solution.py:308
  52.1 0.6 shard_map.167
  52.7 0.5 collective-permute-start.13
  53.1 2.9 %collective-permute-start.12 = (f32[8,64]{1,0:T(8,128)S(1)}, f32[8,64]{1,0:T(8,128)S(1)}, u32[]{:S(2)}, u32[]{:S(2)}) collective-permute-start(f32[8,64]{1,0:T(8,128)S(1)} %get-tuple-element.49.s0), channel_id=1, source_target_pairs={{0,2},{1,3},{2,0},{3,1},{4,6},{5,7},{6,4},{7,5},{8,10},{9,11},{10,... | collective-permute-start | bytes 6152 | tf_op jit(solution)/shard_map/ppermute | solution.py:51
  56.0 0.3 collective-permute-done.13.s3
  56.3 2.5 %collective-permute-start.11 = (f32[8,64]{1,0:T(8,128)S(1)}, f32[8,64]{1,0:T(8,128)S(1)}, u32[]{:S(2)}, u32[]{:S(2)}) collective-permute-start(f32[8,64]{1,0:T(8,128)S(1)} %get-tuple-element.49.s0), channel_id=1, source_target_pairs={{0,1},{1,2},{2,3},{3,0},{4,5},{5,6},{6,7},{7,4},{8,9},{9,10},{10,1... | collective-permute-start | bytes 6152 | tf_op jit(solution)/shard_map/ppermute | solution.py:51
  58.8 1.3 %collective-permute-done.11.s1 = f32[8,64]{1,0:T(8,128)S(1)} collective-permute-done((f32[8,64]{1,0:T(8,128)S(1)}, f32[8,64]{1,0:T(8,128)S(1)}, u32[]{:S(2)}, u32[]{:S(2)}) %collective-permute-start.11) | collective-permute-done | bytes 2080 | tf_op jit(solution)/shard_map/ppermute | solution.py:51
  60.1 0.2 shard_map.168.conv
  60.3 1.7 %shard_map.165 = (f32[64,256]{1,0:T(8,128)S(1)}, f32[64,256]{1,0:T(8,128)S(1)}) custom-call(f32[2]{0:T(128)S(1)} %copy-done.5, bf16[64,256]{1,0:T(8,128)(2,1)S(1)} %get-tuple-element.39.q, bf16[8,64,512]{2,1,0:T(8,128)(2,1)S(1)} %all_to_all.5.mine, bf16[8,64,512]{2,1,0:T(8,128)(2,1)S(1)} %collective-permute-done.3.other), custom_call_target="tpu_custom_call" | custom-call | flops 67108864 | tf_op jit(solution)/shard_map/pallas_call | solution.py:39
  62.1 0.7 shard_map.169
  62.8 2.4 %collective-permute-start.14 = (bf16[64,1024]{1,0:T(8,128)(2,1)S(1)}, bf16[64,1024]{1,0:T(8,128)(2,1)S(1)}, u32[]{:S(2)}, u32[]{:S(2)}) collective-permute-start(bf16[64,1024]{1,0:T(8,128)(2,1)S(1)} %get-tuple-element.51), channel_id=1, source_target_pairs={{0,1},{1,2},{2,3},{3,0},{4,5},{5,6},{6,7},{7,4},{8,9},{9,10},{10,1... | collective-permute-start | bytes 393224 | tf_op jit(solution)/shard_map/ppermute | solution.py:51
  65.2 0.4 collective-permute-start.15
  65.5 2.5 %collective-permute-start.16 = (bf16[64,1024]{1,0:T(8,128)(2,1)S(1)}, bf16[64,1024]{1,0:T(8,128)(2,1)S(1)}, u32[]{:S(2)}, u32[]{:S(2)}) collective-permute-start(bf16[64,1024]{1,0:T(8,128)(2,1)S(1)} %get-tuple-element.53), channel_id=1, source_target_pairs={{0,3},{1,0},{2,1},{3,2},{4,7},{5,4},{6,5},{7,6},{8,11},{9,8},{10,9... | collective-permute-start | bytes 393224 | tf_op jit(solution)/shard_map/ppermute | solution.py:51
  68.1 0.8 %shard_map.170 = (f32[64,512]{1,0:T(8,128)S(1)}, f32[64,512]{1,0:T(8,128)S(1)}) custom-call(bf16[64,2048]{1,0:T(8,128)(2,1)S(1)} %get-tuple-element.54.normed_ref, bf16[2048,512]{1,0:T(8,128)(2,1)S(1)} %copy-done, bf16[2048,512]{1,0:T(8,128)(2,1)S(1)} %copy-done.1), custom_call_target="tpu_custom_call" | custom-call | flops 268435456 | tf_op jit(solution)/shard_map/pallas_call | solution.py:39
  68.9 2.7 %collective-permute-done.15.p2 = bf16[64,1024]{1,0:T(8,128)(2,1)S(1)} collective-permute-done((bf16[64,1024]{1,0:T(8,128)(2,1)S(1)}, bf16[64,1024]{1,0:T(8,128)(2,1)S(1)}, u32[]{:S(2)}, u32[]{:S(2)}) %collective-permute-start.15) | collective-permute-done | bytes 131104 | tf_op jit(solution)/shard_map/ppermute | solution.py:51
  71.6 0.2 shard_map.171
  71.8 1.4 %collective-permute-start.19 = (f32[8,64]{1,0:T(8,128)S(1)}, f32[8,64]{1,0:T(8,128)S(1)}, u32[]{:S(2)}, u32[]{:S(2)}) collective-permute-start(f32[8,64]{1,0:T(8,128)S(1)} %get-tuple-element.58.s0), channel_id=1, source_target_pairs={{0,3},{1,0},{2,1},{3,2},{4,7},{5,4},{6,5},{7,6},{8,11},{9,8},{10,9... | collective-permute-start | bytes 6152 | tf_op jit(solution)/shard_map/ppermute | solution.py:51
  73.2 3.5 %collective-permute-start.18 = (f32[8,64]{1,0:T(8,128)S(1)}, f32[8,64]{1,0:T(8,128)S(1)}, u32[]{:S(2)}, u32[]{:S(2)}) collective-permute-start(f32[8,64]{1,0:T(8,128)S(1)} %get-tuple-element.58.s0), channel_id=1, source_target_pairs={{0,2},{1,3},{2,0},{3,1},{4,6},{5,7},{6,4},{7,5},{8,10},{9,11},{10,... | collective-permute-start | bytes 6152 | tf_op jit(solution)/shard_map/ppermute | solution.py:51
  76.8 1.6 %collective-permute-done.18.s2 = f32[8,64]{1,0:T(8,128)S(1)} collective-permute-done((f32[8,64]{1,0:T(8,128)S(1)}, f32[8,64]{1,0:T(8,128)S(1)}, u32[]{:S(2)}, u32[]{:S(2)}) %collective-permute-start.18) | collective-permute-done | bytes 2080 | tf_op jit(solution)/shard_map/ppermute | solution.py:51
  78.3 2.0 %collective-permute-done.17.s1 = f32[8,64]{1,0:T(8,128)S(1)} collective-permute-done((f32[8,64]{1,0:T(8,128)S(1)}, f32[8,64]{1,0:T(8,128)S(1)}, u32[]{:S(2)}, u32[]{:S(2)}) %collective-permute-start.17) | collective-permute-done | bytes 2080 | tf_op jit(solution)/shard_map/ppermute | solution.py:51
  80.4 0.8 shard_map.172
  (23 shorter events, 0.1 us)
Async XLA Ops:
  0.0 8.0 %collective-permute-start = (bf16[16,2048]{1,0:T(8,128)(2,1)}, bf16[16,2048]{1,0:T(8,128)(2,1)S(1)}, u32[]{:S(2)}, u32[]{:S(2)}) collective-permute-start(bf16[16,2048]{1,0:T(8,128)(2,1)} %refs_0_.1), channel_id=1, source_target_pairs={{0,1},{1,2},{2,3},{3,0},{4,5},{5,6},{6,7},{7,4},{8,9},{9,10},{10,1... | collective-permute-start | bytes 196616 | tf_op jit(solution)/shard_map/ppermute | solution.py:51
  1.3 6.8 %collective-permute-start.2 = (bf16[16,2048]{1,0:T(8,128)(2,1)}, bf16[16,2048]{1,0:T(8,128)(2,1)S(1)}, u32[]{:S(2)}, u32[]{:S(2)}) collective-permute-start(bf16[16,2048]{1,0:T(8,128)(2,1)} %refs_0_.1), channel_id=1, source_target_pairs={{0,3},{1,0},{2,1},{3,2},{4,7},{5,4},{6,5},{7,6},{8,11},{9,8},{10,9... | collective-permute-start | bytes 196616 | tf_op jit(solution)/shard_map/ppermute | solution.py:51
  2.0 6.0 %collective-permute-start.1 = (bf16[16,2048]{1,0:T(8,128)(2,1)}, bf16[16,2048]{1,0:T(8,128)(2,1)S(1)}, u32[]{:S(2)}, u32[]{:S(2)}) collective-permute-start(bf16[16,2048]{1,0:T(8,128)(2,1)} %refs_0_.1), channel_id=1, source_target_pairs={{0,2},{1,3},{2,0},{3,1},{4,6},{5,7},{6,4},{7,5},{8,10},{9,11},{10,... | collective-permute-start | bytes 196616 | tf_op jit(solution)/shard_map/ppermute | solution.py:51
  8.1 26.4 %copy-start.5 = (f32[2]{0:T(128)S(1)}, f32[2]{0:T(128)}, u32[]{:S(2)}) copy-start(f32[2]{0:T(128)} %offset.3) | copy-start | bytes 28
  8.1 54.0 %copy-start.3 = (bf16[256,2048]{1,0:T(8,128)(2,1)S(1)}, bf16[256,2048]{1,0:T(8,128)(2,1)}, u32[]{:S(2)}) copy-start(bf16[256,2048]{1,0:T(8,128)(2,1)} %w_conv.1) | copy-start | bytes 3145732
  9.3 42.8 %copy-start.8 = (f32[31,256]{1,0:T(8,128)S(1)}, f32[31,256]{1,0:T(8,128)}, u32[]{:S(2)}) copy-start(f32[31,256]{1,0:T(8,128)} %taps.1) | copy-start | bytes 95236
  9.3 42.8 %copy-start.9 = (f32[256]{0:T(256)S(1)}, f32[256]{0:T(256)}, u32[]{:S(2)}) copy-start(f32[256]{0:T(256)} %param.28) | copy-start | bytes 3076
  9.3 50.8 %copy-start.6 = (f32[256]{0:T(256)S(1)}, f32[256]{0:T(256)}, u32[]{:S(2)}) copy-start(f32[256]{0:T(256)} %param.29) | copy-start | bytes 3076
  9.3 50.8 %copy-start.7 = (f32[256]{0:T(256)S(1)}, f32[256]{0:T(256)}, u32[]{:S(2)}) copy-start(f32[256]{0:T(256)} %param.30) | copy-start | bytes 3076
  9.3 52.7 %copy-start.2 = (bf16[256,2048]{1,0:T(8,128)(2,1)S(1)}, bf16[256,2048]{1,0:T(8,128)(2,1)}, u32[]{:S(2)}) copy-start(bf16[256,2048]{1,0:T(8,128)(2,1)} %w_attn.1) | copy-start | bytes 3145732
  23.5 11.0 %collective-permute-start.3 = (bf16[8,64,512]{2,1,0:T(8,128)(2,1)S(1)}, bf16[8,64,512]{2,1,0:T(8,128)(2,1)S(1)}, u32[]{:S(2)}, u32[]{:S(2)}) collective-permute-start(bf16[8,64,512]{2,1,0:T(8,128)(2,1)S(1)} %all_to_all.5.mine), channel_id=1, source_target_pairs={{0,4},{4,0},{1,5},{5,1},{2,6},{6,2},{3,7},{7,3},{8,12},{12,8},{9,1... | collective-permute-start | bytes 1572872 | tf_op jit(solution)/shard_map/ppermute | solution.py:331
  23.5 8.7 %collective-permute-start.6 = (bf16[64,256]{1,0:T(8,128)(2,1)S(1)}, bf16[64,256]{1,0:T(8,128)(2,1)S(1)}, u32[]{:S(2)}, u32[]{:S(2)}) collective-permute-start(bf16[64,256]{1,0:T(8,128)(2,1)S(1)} %get-tuple-element.39.q), channel_id=1, source_target_pairs={{192,0},{193,1},{194,2},{195,3},{196,4},{197,5},{198,6},{199,7},{2... | collective-permute-start | bytes 98312 | tf_op jit(solution)/shard_map/ppermute | solution.py:306
  24.8 9.7 %collective-permute-start.5 = (bf16[64,256]{1,0:T(8,128)(2,1)S(1)}, bf16[64,256]{1,0:T(8,128)(2,1)S(1)}, u32[]{:S(2)}, u32[]{:S(2)}) collective-permute-start(bf16[64,256]{1,0:T(8,128)(2,1)S(1)} %get-tuple-element.39.q), channel_id=1, source_target_pairs={{128,0},{192,64},{129,1},{193,65},{130,2},{194,66},{131,3},{195,67... | collective-permute-start | bytes 98312 | tf_op jit(solution)/shard_map/ppermute | solution.py:306
  26.1 8.4 %collective-permute-start.4 = (bf16[64,256]{1,0:T(8,128)(2,1)S(1)}, bf16[64,256]{1,0:T(8,128)(2,1)S(1)}, u32[]{:S(2)}, u32[]{:S(2)}) collective-permute-start(bf16[64,256]{1,0:T(8,128)(2,1)S(1)} %get-tuple-element.39.q), channel_id=1, source_target_pairs={{64,0},{128,64},{192,128},{65,1},{129,65},{193,129},{66,2},{130,66... | collective-permute-start | bytes 98312 | tf_op jit(solution)/shard_map/ppermute | solution.py:306
  34.5 33.6 %copy-start.1 = (bf16[2048,512]{1,0:T(8,128)(2,1)S(1)}, bf16[2048,512]{1,0:T(8,128)(2,1)}, u32[]{:S(2)}) copy-start(bf16[2048,512]{1,0:T(8,128)(2,1)} %wc.1) | copy-start | bytes 6291460
  37.0 31.0 %copy-start = (bf16[2048,512]{1,0:T(8,128)(2,1)S(1)}, bf16[2048,512]{1,0:T(8,128)(2,1)}, u32[]{:S(2)}) copy-start(bf16[2048,512]{1,0:T(8,128)(2,1)} %wa.1) | copy-start | bytes 6291460
  37.0 25.0 %collective-permute-start.7 = (bf16[72,256]{1,0:T(8,128)(2,1)S(1)}, bf16[72,256]{1,0:T(8,128)(2,1)S(1)}, u32[]{:S(2)}, u32[]{:S(2)}) collective-permute-start(bf16[72,256]{1,0:T(8,128)(2,1)S(1)} %get-tuple-element.43), channel_id=1, source_target_pairs={{0,64},{64,128},{128,192},{192,0},{1,65},{65,129},{129,193},{193,1... | collective-permute-start | bytes 110600 | tf_op jit(solution)/shard_map/ppermute | solution.py:344
  40.9 21.1 %collective-permute-start.8 = (bf16[72,256]{1,0:T(8,128)(2,1)S(1)}, bf16[72,256]{1,0:T(8,128)(2,1)S(1)}, u32[]{:S(2)}, u32[]{:S(2)}) collective-permute-start(bf16[72,256]{1,0:T(8,128)(2,1)S(1)} %get-tuple-element.44), channel_id=1, source_target_pairs={{0,128},{64,192},{128,0},{192,64},{1,129},{65,193},{129,1},{193,65... | collective-permute-start | bytes 110600 | tf_op jit(solution)/shard_map/ppermute | solution.py:344
  41.6 20.5 %collective-permute-start.9 = (bf16[72,256]{1,0:T(8,128)(2,1)S(1)}, bf16[72,256]{1,0:T(8,128)(2,1)S(1)}, u32[]{:S(2)}, u32[]{:S(2)}) collective-permute-start(bf16[72,256]{1,0:T(8,128)(2,1)S(1)} %get-tuple-element.45), channel_id=1, source_target_pairs={{0,192},{64,0},{128,64},{192,128},{1,193},{65,1},{129,65},{193,129... | collective-permute-start | bytes 110600 | tf_op jit(solution)/shard_map/ppermute | solution.py:344
  45.6 6.5 %collective-permute-start.10 = (bf16[32,256]{1,0:T(8,128)(2,1)S(1)}, bf16[32,256]{1,0:T(8,128)(2,1)S(1)}, u32[]{:S(2)}, u32[]{:S(2)}) collective-permute-start(bf16[32,256]{1,0:T(8,128)(2,1)S(1)} %get-tuple-element.47), channel_id=1, source_target_pairs={{0,4},{4,8},{8,12},{12,16},{16,20},{20,24},{24,28},{28,32},{32,36}... | collective-permute-start | bytes 49160 | tf_op jit(solution)/shard_map/ppermute | solution.py:308
  52.7 3.6 %collective-permute-start.13 = (f32[8,64]{1,0:T(8,128)S(1)}, f32[8,64]{1,0:T(8,128)S(1)}, u32[]{:S(2)}, u32[]{:S(2)}) collective-permute-start(f32[8,64]{1,0:T(8,128)S(1)} %get-tuple-element.49.s0), channel_id=1, source_target_pairs={{0,3},{1,0},{2,1},{3,2},{4,7},{5,4},{6,5},{7,6},{8,11},{9,8},{10,9... | collective-permute-start | bytes 6152 | tf_op jit(solution)/shard_map/ppermute | solution.py:51
  53.1 5.7 %collective-permute-start.12 = (f32[8,64]{1,0:T(8,128)S(1)}, f32[8,64]{1,0:T(8,128)S(1)}, u32[]{:S(2)}, u32[]{:S(2)}) collective-permute-start(f32[8,64]{1,0:T(8,128)S(1)} %get-tuple-element.49.s0), channel_id=1, source_target_pairs={{0,2},{1,3},{2,0},{3,1},{4,6},{5,7},{6,4},{7,5},{8,10},{9,11},{10,... | collective-permute-start | bytes 6152 | tf_op jit(solution)/shard_map/ppermute | solution.py:51
  56.3 3.8 %collective-permute-start.11 = (f32[8,64]{1,0:T(8,128)S(1)}, f32[8,64]{1,0:T(8,128)S(1)}, u32[]{:S(2)}, u32[]{:S(2)}) collective-permute-start(f32[8,64]{1,0:T(8,128)S(1)} %get-tuple-element.49.s0), channel_id=1, source_target_pairs={{0,1},{1,2},{2,3},{3,0},{4,5},{5,6},{6,7},{7,4},{8,9},{9,10},{10,1... | collective-permute-start | bytes 6152 | tf_op jit(solution)/shard_map/ppermute | solution.py:51
  62.8 6.2 %collective-permute-start.14 = (bf16[64,1024]{1,0:T(8,128)(2,1)S(1)}, bf16[64,1024]{1,0:T(8,128)(2,1)S(1)}, u32[]{:S(2)}, u32[]{:S(2)}) collective-permute-start(bf16[64,1024]{1,0:T(8,128)(2,1)S(1)} %get-tuple-element.51), channel_id=1, source_target_pairs={{0,1},{1,2},{2,3},{3,0},{4,5},{5,6},{6,7},{7,4},{8,9},{9,10},{10,1... | collective-permute-start | bytes 393224 | tf_op jit(solution)/shard_map/ppermute | solution.py:51
  65.2 6.5 %collective-permute-start.15 = (bf16[64,1024]{1,0:T(8,128)(2,1)S(1)}, bf16[64,1024]{1,0:T(8,128)(2,1)S(1)}, u32[]{:S(2)}, u32[]{:S(2)}) collective-permute-start(bf16[64,1024]{1,0:T(8,128)(2,1)S(1)} %get-tuple-element.52), channel_id=1, source_target_pairs={{0,2},{1,3},{2,0},{3,1},{4,6},{5,7},{6,4},{7,5},{8,10},{9,11},{10,... | collective-permute-start | bytes 393224 | tf_op jit(solution)/shard_map/ppermute | solution.py:51
  65.5 6.1 %collective-permute-start.16 = (bf16[64,1024]{1,0:T(8,128)(2,1)S(1)}, bf16[64,1024]{1,0:T(8,128)(2,1)S(1)}, u32[]{:S(2)}, u32[]{:S(2)}) collective-permute-start(bf16[64,1024]{1,0:T(8,128)(2,1)S(1)} %get-tuple-element.53), channel_id=1, source_target_pairs={{0,3},{1,0},{2,1},{3,2},{4,7},{5,4},{6,5},{7,6},{8,11},{9,8},{10,9... | collective-permute-start | bytes 393224 | tf_op jit(solution)/shard_map/ppermute | solution.py:51
  68.1 12.3 %copy-start.4 = (f32[512]{0:T(512)S(1)}, f32[512]{0:T(512)}, u32[]{:S(2)}) copy-start(f32[512]{0:T(512)} %param.33) | copy-start | bytes 6148
  71.8 4.9 %collective-permute-start.19 = (f32[8,64]{1,0:T(8,128)S(1)}, f32[8,64]{1,0:T(8,128)S(1)}, u32[]{:S(2)}, u32[]{:S(2)}) collective-permute-start(f32[8,64]{1,0:T(8,128)S(1)} %get-tuple-element.58.s0), channel_id=1, source_target_pairs={{0,3},{1,0},{2,1},{3,2},{4,7},{5,4},{6,5},{7,6},{8,11},{9,8},{10,9... | collective-permute-start | bytes 6152 | tf_op jit(solution)/shard_map/ppermute | solution.py:51
  73.2 5.1 %collective-permute-start.18 = (f32[8,64]{1,0:T(8,128)S(1)}, f32[8,64]{1,0:T(8,128)S(1)}, u32[]{:S(2)}, u32[]{:S(2)}) collective-permute-start(f32[8,64]{1,0:T(8,128)S(1)} %get-tuple-element.58.s0), channel_id=1, source_target_pairs={{0,2},{1,3},{2,0},{3,1},{4,6},{5,7},{6,4},{7,5},{8,10},{9,11},{10,... | collective-permute-start | bytes 6152 | tf_op jit(solution)/shard_map/ppermute | solution.py:51
  76.8 3.6 %collective-permute-start.17 = (f32[8,64]{1,0:T(8,128)S(1)}, f32[8,64]{1,0:T(8,128)S(1)}, u32[]{:S(2)}, u32[]{:S(2)}) collective-permute-start(f32[8,64]{1,0:T(8,128)S(1)} %get-tuple-element.58.s0), channel_id=1, source_target_pairs={{0,1},{1,2},{2,3},{3,0},{4,5},{5,6},{6,7},{7,4},{8,9},{9,10},{10,1... | collective-permute-start | bytes 6152 | tf_op jit(solution)/shard_map/ppermute | solution.py:51

commit v3 on v2

--- a/solution.py
+++ b/solution.py
@@ -121,8 +121,14 @@
     padded[HALO : HALO + rows, :] = gated_ref[...].astype(F32)
     total = jnp.broadcast_to(bias[...], (rows, bias.shape[1]))
     first = HALO - (WIDTH - 1)
-    for i in range(WIDTH):
-        total = total + taps[i : i + 1, :] * padded[first + i : first + i + rows, :]
+    for shift in range(8):
+        span = rows if shift == 0 else rows + 8
+        part = 0.0
+        for i in range(WIDTH):
+            if (first + i) % 8 == shift:
+                start = first + i - shift
+                part = part + taps[i : i + 1, :] * padded[start : start + span, :]
+        total = total + part[shift : shift + rows, :]
     conv_out[...] = total
     mean = jnp.mean(total, axis=1, keepdims=True)
     centered = total - mean

time: 81.3 us -> 81.2 us (level)
  no operation moved by 1% of the time
where the time goes in v3:
time: 81.2 us; the launch traced here: 81 us
  starting transfers between devices  33.8 us (42%)
  waiting for transfers between devices  21.5 us (26%)
  blocking collectives  14.1 us (17%)
  Pallas kernels  11.3 us (14%)
    ppermute x12, starting transfers between devices, to_rotated(): lax.ppermute(piece, 'tp', [(i, (i + d) % N_TP) for i in range(N_TP)])  21.3 us
    all_to_all x1, blocking collectives, on_device(): kv_mine = lax.all_to_all(kv, ('zl', 'x'), 0, 0)  14.1 us
    pallas_call x10, Pallas kernels, pallas_call(): pl.pallas_call(body, out_shape=[out_space(shape, dtype) for shape, dtype...  11.3 us
    ppermute x3, starting transfers between devices, on_device(): lax.ppermute(m, 'zh', [(i, (i + d) % N_ZH) for i in range(N_ZH)])  8.56 us
    ppermute x12, waiting for transfers between devices, to_rotated(): lax.ppermute(piece, 'tp', [(i, (i + d) % N_TP) for i in range(N_TP)])  7.91 us
    ppermute x3, waiting for transfers between devices, on_device(): lax.ppermute(q, 'zh', [(i, i - d) for i in range(d, N_ZH)])  7.12 us
    ppermute x1, waiting for transfers between devices, on_device(): lax.ppermute(tail, SP, [(i, (i + 1) % count) for i in range(count)])  6.48 us
    ppermute x3, starting transfers between devices, on_device(): lax.ppermute(q, 'zh', [(i, i - d) for i in range(d, N_ZH)])  3.87 us
  transfers between devices with their start and end apart: 20, of which 8 were waited for; matrix products, arithmetic and copies ran while one was open for 0% of the time, Pallas kernels for 7%

profile of v3, /device:TPU:16, one launch (start us, length us, event | category | flops | bytes accessed | tf_op | source)
XLA Modules:
  0.0 81.0 jit_solution(14273785834214108545)
XLA Ops:
  0.0 1.3 %collective-permute-start = (bf16[16,2048]{1,0:T(8,128)(2,1)}, bf16[16,2048]{1,0:T(8,128)(2,1)S(1)}, u32[]{:S(2)}, u32[]{:S(2)}) collective-permute-start(bf16[16,2048]{1,0:T(8,128)(2,1)} %refs_0_.1), channel_id=1, source_target_pairs={{0,1},{1,2},{2,3},{3,0},{4,5},{5,6},{6,7},{7,4},{8,9},{9,10},{10,1... | collective-permute-start | bytes 196616 | tf_op jit(solution)/shard_map/ppermute | solution.py:51
  1.3 0.7 collective-permute-start.2
  2.0 3.3 %collective-permute-start.1 = (bf16[16,2048]{1,0:T(8,128)(2,1)}, bf16[16,2048]{1,0:T(8,128)(2,1)S(1)}, u32[]{:S(2)}, u32[]{:S(2)}) collective-permute-start(bf16[16,2048]{1,0:T(8,128)(2,1)} %refs_0_.1), channel_id=1, source_target_pairs={{0,2},{1,3},{2,0},{3,1},{4,6},{5,7},{6,4},{7,5},{8,10},{9,11},{10,... | collective-permute-start | bytes 196616 | tf_op jit(solution)/shard_map/ppermute | solution.py:51
  5.3 2.7 %shard_map.163 = (bf16[16,2048]{1,0:T(8,128)(2,1)S(1)}, f32[1,2048]{1,0:T(1,128)S(1)}, bf16[2048,256]{1,0:T(8,128)(2,1)S(1)}, bf16[2048,256]{1,0:T(8,128)(2,1)S(...) custom-call(bf16[16,2048]{1,0:T(8,128)(2,1)} %refs_0_.1, ...), custom_call_target="tpu_custom_call" | custom-call | flops 10000000 | tf_op jit(solution)/shard_map/pallas_call | solution.py:39
  8.0 0.0 collective-permute-done.2.x3
  8.1 0.0 collective-permute-done.1.x2
  8.1 0.0 copy-start.5
  8.1 0.0 copy-start.3
  8.1 1.2 %shard_map.164 = (bf16[8,64,512]{2,1,0:T(8,128)(2,1)S(1)}, bf16[64,256]{1,0:T(8,128)(2,1)S(1)}, bf16[64,2048]{1,0:T(8,128)(2,1)S(1)}, bf16[64,256]{1,0:T(8,128)(2,1)S(1)}, bf16[32,256]{1,0:T(8,128)(2,1)S(1)}) custom-call(bf16[16,2048]{1,0:T(8,128)(2,1)S(1)} %get-tuple-element.32.x0, bf16[16,2048]{1,0:T(8,128)(2,1)S(1)} %collective-permute-done.x1, ...), custom_call_target="tpu_custom_call" | custom-call | flops 201326592 | tf_op jit(solution)/shard_map/pallas_call | solution.py:39
  9.3 0.0 copy-start.8
  9.3 0.0 copy-start.9
  9.3 0.0 copy-start.6
  9.3 0.0 copy-start.7
  9.3 0.0 copy-start.2
  9.3 14.1 %all_to_all.5.mine = bf16[8,64,512]{2,1,0:T(8,128)(2,1)S(1)} all-to-all(bf16[8,64,512]{2,1,0:T(8,128)(2,1)S(1)} %get-tuple-element.40), channel_id=1, replica_groups=mesh['zh'=4,'zl'=2,'x'=4,'c'=2,'tp'=4] {'zl','x'}, dimensions={0} | all-to-all | bytes 1048576 | tf_op jit(solution)/shard_map/all_to_all | solution.py:311
  23.5 1.3 %collective-permute-start.6 = (bf16[64,256]{1,0:T(8,128)(2,1)S(1)}, bf16[64,256]{1,0:T(8,128)(2,1)S(1)}, u32[]{:S(2)}, u32[]{:S(2)}) collective-permute-start(bf16[64,256]{1,0:T(8,128)(2,1)S(1)} %get-tuple-element.39.q), channel_id=1, source_target_pairs={{192,0},{193,1},{194,2},{195,3},{196,4},{197,5},{198,6},{199,7},{2... | collective-permute-start | bytes 98312 | tf_op jit(solution)/shard_map/ppermute | solution.py:312
  24.8 1.3 %collective-permute-start.5 = (bf16[64,256]{1,0:T(8,128)(2,1)S(1)}, bf16[64,256]{1,0:T(8,128)(2,1)S(1)}, u32[]{:S(2)}, u32[]{:S(2)}) collective-permute-start(bf16[64,256]{1,0:T(8,128)(2,1)S(1)} %get-tuple-element.39.q), channel_id=1, source_target_pairs={{128,0},{192,64},{129,1},{193,65},{130,2},{194,66},{131,3},{195,67... | collective-permute-start | bytes 98312 | tf_op jit(solution)/shard_map/ppermute | solution.py:312
  26.1 1.3 %collective-permute-start.4 = (bf16[64,256]{1,0:T(8,128)(2,1)S(1)}, bf16[64,256]{1,0:T(8,128)(2,1)S(1)}, u32[]{:S(2)}, u32[]{:S(2)}) collective-permute-start(bf16[64,256]{1,0:T(8,128)(2,1)S(1)} %get-tuple-element.39.q), channel_id=1, source_target_pairs={{64,0},{128,64},{192,128},{65,1},{129,65},{193,129},{66,2},{130,66... | collective-permute-start | bytes 98312 | tf_op jit(solution)/shard_map/ppermute | solution.py:312
  27.4 4.8 %collective-permute-done.6.q3 = bf16[64,256]{1,0:T(8,128)(2,1)S(1)} collective-permute-done((bf16[64,256]{1,0:T(8,128)(2,1)S(1)}, bf16[64,256]{1,0:T(8,128)(2,1)S(1)}, u32[]{:S(2)}, u32[]{:S(2)}) %collective-permute-start.6) | collective-permute-done | bytes 32800 | tf_op jit(solution)/shard_map/ppermute | solution.py:312
  32.2 2.3 %collective-permute-done.5.q2 = bf16[64,256]{1,0:T(8,128)(2,1)S(1)} collective-permute-done((bf16[64,256]{1,0:T(8,128)(2,1)S(1)}, bf16[64,256]{1,0:T(8,128)(2,1)S(1)}, u32[]{:S(2)}, u32[]{:S(2)}) %collective-permute-start.5) | collective-permute-done | bytes 32800 | tf_op jit(solution)/shard_map/ppermute | solution.py:312
  34.5 0.0 collective-permute-done.4.q1
  34.5 0.0 copy-start.1
  34.5 2.5 %shard_map.166 = (bf16[72,256]{1,0:T(8,128)(2,1)S(1)}, bf16[72,256]{1,0:T(8,128)(2,1)S(1)}, bf16[72,256]{1,0:T(8,128)(2,1)S(1)}) custom-call(f32[2]{0:T(128)S(1)} %copy-done.5, bf16[64,256]{1,0:T(8,128)(2,1)S(1)} %collective-permute-done.4.q1, bf16[64,256]{1,0:T(8,128)(2,1)S(1)} %collective-permute-done.5.q2, bf16[64,256]{1,0:T(8,128)(2,1)S(1)} %collective-permute-done.6.q3, ...), custom_call_target="tpu_custom_call" | custom-call | flops 201326592 | tf_op jit(solution)/shard_map/pallas_call | solution.py:39
  37.0 0.0 copy-start
  37.0 3.8 %collective-permute-start.7 = (bf16[72,256]{1,0:T(8,128)(2,1)S(1)}, bf16[72,256]{1,0:T(8,128)(2,1)S(1)}, u32[]{:S(2)}, u32[]{:S(2)}) collective-permute-start(bf16[72,256]{1,0:T(8,128)(2,1)S(1)} %get-tuple-element.43), channel_id=1, source_target_pairs={{0,64},{64,128},{128,192},{192,0},{1,65},{65,129},{129,193},{193,1... | collective-permute-start | bytes 110600 | tf_op jit(solution)/shard_map/ppermute | solution.py:350
  40.9 0.7 collective-permute-start.8
  41.6 4.0 %collective-permute-start.9 = (bf16[72,256]{1,0:T(8,128)(2,1)S(1)}, bf16[72,256]{1,0:T(8,128)(2,1)S(1)}, u32[]{:S(2)}, u32[]{:S(2)}) collective-permute-start(bf16[72,256]{1,0:T(8,128)(2,1)S(1)} %get-tuple-element.45), channel_id=1, source_target_pairs={{0,192},{64,0},{128,64},{192,128},{1,193},{65,1},{129,65},{193,129... | collective-permute-start | bytes 110600 | tf_op jit(solution)/shard_map/ppermute | solution.py:350
  45.6 6.5 %collective-permute-done.10.tail_ref = bf16[32,256]{1,0:T(8,128)(2,1)S(1)} collective-permute-done((bf16[32,256]{1,0:T(8,128)(2,1)S(1)}, bf16[32,256]{1,0:T(8,128)(2,1)S(1)}, u32[]{:S(2)}, u32[]{:S(2)}) %collective-permute-start.10) | collective-permute-done | bytes 16416 | tf_op jit(solution)/shard_map/ppermute | solution.py:314
  52.1 0.4 shard_map.167
  52.5 0.5 collective-permute-start.13
  53.0 2.9 %collective-permute-start.12 = (f32[8,64]{1,0:T(8,128)S(1)}, f32[8,64]{1,0:T(8,128)S(1)}, u32[]{:S(2)}, u32[]{:S(2)}) collective-permute-start(f32[8,64]{1,0:T(8,128)S(1)} %get-tuple-element.49.s0), channel_id=1, source_target_pairs={{0,2},{1,3},{2,0},{3,1},{4,6},{5,7},{6,4},{7,5},{8,10},{9,11},{10,... | collective-permute-start | bytes 6152 | tf_op jit(solution)/shard_map/ppermute | solution.py:51
  55.9 0.3 collective-permute-done.13.s3
  56.1 2.5 %collective-permute-start.11 = (f32[8,64]{1,0:T(8,128)S(1)}, f32[8,64]{1,0:T(8,128)S(1)}, u32[]{:S(2)}, u32[]{:S(2)}) collective-permute-start(f32[8,64]{1,0:T(8,128)S(1)} %get-tuple-element.49.s0), channel_id=1, source_target_pairs={{0,1},{1,2},{2,3},{3,0},{4,5},{5,6},{6,7},{7,4},{8,9},{9,10},{10,1... | collective-permute-start | bytes 6152 | tf_op jit(solution)/shard_map/ppermute | solution.py:51
  58.6 1.3 %collective-permute-done.11.s1 = f32[8,64]{1,0:T(8,128)S(1)} collective-permute-done((f32[8,64]{1,0:T(8,128)S(1)}, f32[8,64]{1,0:T(8,128)S(1)}, u32[]{:S(2)}, u32[]{:S(2)}) %collective-permute-start.11) | collective-permute-done | bytes 2080 | tf_op jit(solution)/shard_map/ppermute | solution.py:51
  59.9 0.2 shard_map.168.conv
  60.2 1.7 %shard_map.165 = (f32[64,256]{1,0:T(8,128)S(1)}, f32[64,256]{1,0:T(8,128)S(1)}) custom-call(f32[2]{0:T(128)S(1)} %copy-done.5, bf16[64,256]{1,0:T(8,128)(2,1)S(1)} %get-tuple-element.39.q, bf16[8,64,512]{2,1,0:T(8,128)(2,1)S(1)} %all_to_all.5.mine, bf16[8,64,512]{2,1,0:T(8,128)(2,1)S(1)} %collective-permute-done.3.other), custom_call_target="tpu_custom_call" | custom-call | flops 67108864 | tf_op jit(solution)/shard_map/pallas_call | solution.py:39
  61.9 0.7 shard_map.169
  62.6 2.4 %collective-permute-start.14 = (bf16[64,1024]{1,0:T(8,128)(2,1)S(1)}, bf16[64,1024]{1,0:T(8,128)(2,1)S(1)}, u32[]{:S(2)}, u32[]{:S(2)}) collective-permute-start(bf16[64,1024]{1,0:T(8,128)(2,1)S(1)} %get-tuple-element.51), channel_id=1, source_target_pairs={{0,1},{1,2},{2,3},{3,0},{4,5},{5,6},{6,7},{7,4},{8,9},{9,10},{10,1... | collective-permute-start | bytes 393224 | tf_op jit(solution)/shard_map/ppermute | solution.py:51
  65.0 0.4 collective-permute-start.15
  65.3 2.5 %collective-permute-start.16 = (bf16[64,1024]{1,0:T(8,128)(2,1)S(1)}, bf16[64,1024]{1,0:T(8,128)(2,1)S(1)}, u32[]{:S(2)}, u32[]{:S(2)}) collective-permute-start(bf16[64,1024]{1,0:T(8,128)(2,1)S(1)} %get-tuple-element.53), channel_id=1, source_target_pairs={{0,3},{1,0},{2,1},{3,2},{4,7},{5,4},{6,5},{7,6},{8,11},{9,8},{10,9... | collective-permute-start | bytes 393224 | tf_op jit(solution)/shard_map/ppermute | solution.py:51
  67.9 0.8 %shard_map.170 = (f32[64,512]{1,0:T(8,128)S(1)}, f32[64,512]{1,0:T(8,128)S(1)}) custom-call(bf16[64,2048]{1,0:T(8,128)(2,1)S(1)} %get-tuple-element.54.normed_ref, bf16[2048,512]{1,0:T(8,128)(2,1)S(1)} %copy-done, bf16[2048,512]{1,0:T(8,128)(2,1)S(1)} %copy-done.1), custom_call_target="tpu_custom_call" | custom-call | flops 268435456 | tf_op jit(solution)/shard_map/pallas_call | solution.py:39
  68.7 2.7 %collective-permute-done.15.p2 = bf16[64,1024]{1,0:T(8,128)(2,1)S(1)} collective-permute-done((bf16[64,1024]{1,0:T(8,128)(2,1)S(1)}, bf16[64,1024]{1,0:T(8,128)(2,1)S(1)}, u32[]{:S(2)}, u32[]{:S(2)}) %collective-permute-start.15) | collective-permute-done | bytes 131104 | tf_op jit(solution)/shard_map/ppermute | solution.py:51
  71.5 0.2 shard_map.171
  71.7 1.4 %collective-permute-start.19 = (f32[8,64]{1,0:T(8,128)S(1)}, f32[8,64]{1,0:T(8,128)S(1)}, u32[]{:S(2)}, u32[]{:S(2)}) collective-permute-start(f32[8,64]{1,0:T(8,128)S(1)} %get-tuple-element.58.s0), channel_id=1, source_target_pairs={{0,3},{1,0},{2,1},{3,2},{4,7},{5,4},{6,5},{7,6},{8,11},{9,8},{10,9... | collective-permute-start | bytes 6152 | tf_op jit(solution)/shard_map/ppermute | solution.py:51
  73.1 3.5 %collective-permute-start.18 = (f32[8,64]{1,0:T(8,128)S(1)}, f32[8,64]{1,0:T(8,128)S(1)}, u32[]{:S(2)}, u32[]{:S(2)}) collective-permute-start(f32[8,64]{1,0:T(8,128)S(1)} %get-tuple-element.58.s0), channel_id=1, source_target_pairs={{0,2},{1,3},{2,0},{3,1},{4,6},{5,7},{6,4},{7,5},{8,10},{9,11},{10,... | collective-permute-start | bytes 6152 | tf_op jit(solution)/shard_map/ppermute | solution.py:51
  76.6 1.6 %collective-permute-done.18.s2 = f32[8,64]{1,0:T(8,128)S(1)} collective-permute-done((f32[8,64]{1,0:T(8,128)S(1)}, f32[8,64]{1,0:T(8,128)S(1)}, u32[]{:S(2)}, u32[]{:S(2)}) %collective-permute-start.18) | collective-permute-done | bytes 2080 | tf_op jit(solution)/shard_map/ppermute | solution.py:51
  78.2 2.0 %collective-permute-done.17.s1 = f32[8,64]{1,0:T(8,128)S(1)} collective-permute-done((f32[8,64]{1,0:T(8,128)S(1)}, f32[8,64]{1,0:T(8,128)S(1)}, u32[]{:S(2)}, u32[]{:S(2)}) %collective-permute-start.17) | collective-permute-done | bytes 2080 | tf_op jit(solution)/shard_map/ppermute | solution.py:51
  80.2 0.8 shard_map.172
  (23 shorter events, 0.1 us)
Async XLA Ops:
  0.0 8.0 %collective-permute-start = (bf16[16,2048]{1,0:T(8,128)(2,1)}, bf16[16,2048]{1,0:T(8,128)(2,1)S(1)}, u32[]{:S(2)}, u32[]{:S(2)}) collective-permute-start(bf16[16,2048]{1,0:T(8,128)(2,1)} %refs_0_.1), channel_id=1, source_target_pairs={{0,1},{1,2},{2,3},{3,0},{4,5},{5,6},{6,7},{7,4},{8,9},{9,10},{10,1... | collective-permute-start | bytes 196616 | tf_op jit(solution)/shard_map/ppermute | solution.py:51
  1.3 6.8 %collective-permute-start.2 = (bf16[16,2048]{1,0:T(8,128)(2,1)}, bf16[16,2048]{1,0:T(8,128)(2,1)S(1)}, u32[]{:S(2)}, u32[]{:S(2)}) collective-permute-start(bf16[16,2048]{1,0:T(8,128)(2,1)} %refs_0_.1), channel_id=1, source_target_pairs={{0,3},{1,0},{2,1},{3,2},{4,7},{5,4},{6,5},{7,6},{8,11},{9,8},{10,9... | collective-permute-start | bytes 196616 | tf_op jit(solution)/shard_map/ppermute | solution.py:51
  2.0 6.0 %collective-permute-start.1 = (bf16[16,2048]{1,0:T(8,128)(2,1)}, bf16[16,2048]{1,0:T(8,128)(2,1)S(1)}, u32[]{:S(2)}, u32[]{:S(2)}) collective-permute-start(bf16[16,2048]{1,0:T(8,128)(2,1)} %refs_0_.1), channel_id=1, source_target_pairs={{0,2},{1,3},{2,0},{3,1},{4,6},{5,7},{6,4},{7,5},{8,10},{9,11},{10,... | collective-permute-start | bytes 196616 | tf_op jit(solution)/shard_map/ppermute | solution.py:51
  8.1 26.4 %copy-start.5 = (f32[2]{0:T(128)S(1)}, f32[2]{0:T(128)}, u32[]{:S(2)}) copy-start(f32[2]{0:T(128)} %offset.3) | copy-start | bytes 28
  8.1 53.8 %copy-start.3 = (bf16[256,2048]{1,0:T(8,128)(2,1)S(1)}, bf16[256,2048]{1,0:T(8,128)(2,1)}, u32[]{:S(2)}) copy-start(bf16[256,2048]{1,0:T(8,128)(2,1)} %w_conv.1) | copy-start | bytes 3145732
  9.3 42.8 %copy-start.8 = (f32[31,256]{1,0:T(8,128)S(1)}, f32[31,256]{1,0:T(8,128)}, u32[]{:S(2)}) copy-start(f32[31,256]{1,0:T(8,128)} %taps.1) | copy-start | bytes 95236
  9.3 42.8 %copy-start.9 = (f32[256]{0:T(256)S(1)}, f32[256]{0:T(256)}, u32[]{:S(2)}) copy-start(f32[256]{0:T(256)} %param.28) | copy-start | bytes 3076
  9.3 50.6 %copy-start.6 = (f32[256]{0:T(256)S(1)}, f32[256]{0:T(256)}, u32[]{:S(2)}) copy-start(f32[256]{0:T(256)} %param.29) | copy-start | bytes 3076
  9.3 50.6 %copy-start.7 = (f32[256]{0:T(256)S(1)}, f32[256]{0:T(256)}, u32[]{:S(2)}) copy-start(f32[256]{0:T(256)} %param.30) | copy-start | bytes 3076
  9.3 52.5 %copy-start.2 = (bf16[256,2048]{1,0:T(8,128)(2,1)S(1)}, bf16[256,2048]{1,0:T(8,128)(2,1)}, u32[]{:S(2)}) copy-start(bf16[256,2048]{1,0:T(8,128)(2,1)} %w_attn.1) | copy-start | bytes 3145732
  23.5 11.0 %collective-permute-start.3 = (bf16[8,64,512]{2,1,0:T(8,128)(2,1)S(1)}, bf16[8,64,512]{2,1,0:T(8,128)(2,1)S(1)}, u32[]{:S(2)}, u32[]{:S(2)}) collective-permute-start(bf16[8,64,512]{2,1,0:T(8,128)(2,1)S(1)} %all_to_all.5.mine), channel_id=1, source_target_pairs={{0,4},{4,0},{1,5},{5,1},{2,6},{6,2},{3,7},{7,3},{8,12},{12,8},{9,1... | collective-permute-start | bytes 1572872 | tf_op jit(solution)/shard_map/ppermute | solution.py:337
  23.5 8.7 %collective-permute-start.6 = (bf16[64,256]{1,0:T(8,128)(2,1)S(1)}, bf16[64,256]{1,0:T(8,128)(2,1)S(1)}, u32[]{:S(2)}, u32[]{:S(2)}) collective-permute-start(bf16[64,256]{1,0:T(8,128)(2,1)S(1)} %get-tuple-element.39.q), channel_id=1, source_target_pairs={{192,0},{193,1},{194,2},{195,3},{196,4},{197,5},{198,6},{199,7},{2... | collective-permute-start | bytes 98312 | tf_op jit(solution)/shard_map/ppermute | solution.py:312
  24.8 9.7 %collective-permute-start.5 = (bf16[64,256]{1,0:T(8,128)(2,1)S(1)}, bf16[64,256]{1,0:T(8,128)(2,1)S(1)}, u32[]{:S(2)}, u32[]{:S(2)}) collective-permute-start(bf16[64,256]{1,0:T(8,128)(2,1)S(1)} %get-tuple-element.39.q), channel_id=1, source_target_pairs={{128,0},{192,64},{129,1},{193,65},{130,2},{194,66},{131,3},{195,67... | collective-permute-start | bytes 98312 | tf_op jit(solution)/shard_map/ppermute | solution.py:312
  26.1 8.4 %collective-permute-start.4 = (bf16[64,256]{1,0:T(8,128)(2,1)S(1)}, bf16[64,256]{1,0:T(8,128)(2,1)S(1)}, u32[]{:S(2)}, u32[]{:S(2)}) collective-permute-start(bf16[64,256]{1,0:T(8,128)(2,1)S(1)} %get-tuple-element.39.q), channel_id=1, source_target_pairs={{64,0},{128,64},{192,128},{65,1},{129,65},{193,129},{66,2},{130,66... | collective-permute-start | bytes 98312 | tf_op jit(solution)/shard_map/ppermute | solution.py:312
  34.5 33.4 %copy-start.1 = (bf16[2048,512]{1,0:T(8,128)(2,1)S(1)}, bf16[2048,512]{1,0:T(8,128)(2,1)}, u32[]{:S(2)}) copy-start(bf16[2048,512]{1,0:T(8,128)(2,1)} %wc.1) | copy-start | bytes 6291460
  37.0 30.9 %copy-start = (bf16[2048,512]{1,0:T(8,128)(2,1)S(1)}, bf16[2048,512]{1,0:T(8,128)(2,1)}, u32[]{:S(2)}) copy-start(bf16[2048,512]{1,0:T(8,128)(2,1)} %wa.1) | copy-start | bytes 6291460
  37.0 24.8 %collective-permute-start.7 = (bf16[72,256]{1,0:T(8,128)(2,1)S(1)}, bf16[72,256]{1,0:T(8,128)(2,1)S(1)}, u32[]{:S(2)}, u32[]{:S(2)}) collective-permute-start(bf16[72,256]{1,0:T(8,128)(2,1)S(1)} %get-tuple-element.43), channel_id=1, source_target_pairs={{0,64},{64,128},{128,192},{192,0},{1,65},{65,129},{129,193},{193,1... | collective-permute-start | bytes 110600 | tf_op jit(solution)/shard_map/ppermute | solution.py:350
  40.9 21.0 %collective-permute-start.8 = (bf16[72,256]{1,0:T(8,128)(2,1)S(1)}, bf16[72,256]{1,0:T(8,128)(2,1)S(1)}, u32[]{:S(2)}, u32[]{:S(2)}) collective-permute-start(bf16[72,256]{1,0:T(8,128)(2,1)S(1)} %get-tuple-element.44), channel_id=1, source_target_pairs={{0,128},{64,192},{128,0},{192,64},{1,129},{65,193},{129,1},{193,65... | collective-permute-start | bytes 110600 | tf_op jit(solution)/shard_map/ppermute | solution.py:350
  41.6 20.3 %collective-permute-start.9 = (bf16[72,256]{1,0:T(8,128)(2,1)S(1)}, bf16[72,256]{1,0:T(8,128)(2,1)S(1)}, u32[]{:S(2)}, u32[]{:S(2)}) collective-permute-start(bf16[72,256]{1,0:T(8,128)(2,1)S(1)} %get-tuple-element.45), channel_id=1, source_target_pairs={{0,192},{64,0},{128,64},{192,128},{1,193},{65,1},{129,65},{193,129... | collective-permute-start | bytes 110600 | tf_op jit(solution)/shard_map/ppermute | solution.py:350
  45.6 6.5 %collective-permute-start.10 = (bf16[32,256]{1,0:T(8,128)(2,1)S(1)}, bf16[32,256]{1,0:T(8,128)(2,1)S(1)}, u32[]{:S(2)}, u32[]{:S(2)}) collective-permute-start(bf16[32,256]{1,0:T(8,128)(2,1)S(1)} %get-tuple-element.47), channel_id=1, source_target_pairs={{0,4},{4,8},{8,12},{12,16},{16,20},{20,24},{24,28},{28,32},{32,36}... | collective-permute-start | bytes 49160 | tf_op jit(solution)/shard_map/ppermute | solution.py:314
  52.5 3.6 %collective-permute-start.13 = (f32[8,64]{1,0:T(8,128)S(1)}, f32[8,64]{1,0:T(8,128)S(1)}, u32[]{:S(2)}, u32[]{:S(2)}) collective-permute-start(f32[8,64]{1,0:T(8,128)S(1)} %get-tuple-element.49.s0), channel_id=1, source_target_pairs={{0,3},{1,0},{2,1},{3,2},{4,7},{5,4},{6,5},{7,6},{8,11},{9,8},{10,9... | collective-permute-start | bytes 6152 | tf_op jit(solution)/shard_map/ppermute | solution.py:51
  53.0 5.7 %collective-permute-start.12 = (f32[8,64]{1,0:T(8,128)S(1)}, f32[8,64]{1,0:T(8,128)S(1)}, u32[]{:S(2)}, u32[]{:S(2)}) collective-permute-start(f32[8,64]{1,0:T(8,128)S(1)} %get-tuple-element.49.s0), channel_id=1, source_target_pairs={{0,2},{1,3},{2,0},{3,1},{4,6},{5,7},{6,4},{7,5},{8,10},{9,11},{10,... | collective-permute-start | bytes 6152 | tf_op jit(solution)/shard_map/ppermute | solution.py:51
  56.1 3.8 %collective-permute-start.11 = (f32[8,64]{1,0:T(8,128)S(1)}, f32[8,64]{1,0:T(8,128)S(1)}, u32[]{:S(2)}, u32[]{:S(2)}) collective-permute-start(f32[8,64]{1,0:T(8,128)S(1)} %get-tuple-element.49.s0), channel_id=1, source_target_pairs={{0,1},{1,2},{2,3},{3,0},{4,5},{5,6},{6,7},{7,4},{8,9},{9,10},{10,1... | collective-permute-start | bytes 6152 | tf_op jit(solution)/shard_map/ppermute | solution.py:51
  62.6 6.2 %collective-permute-start.14 = (bf16[64,1024]{1,0:T(8,128)(2,1)S(1)}, bf16[64,1024]{1,0:T(8,128)(2,1)S(1)}, u32[]{:S(2)}, u32[]{:S(2)}) collective-permute-start(bf16[64,1024]{1,0:T(8,128)(2,1)S(1)} %get-tuple-element.51), channel_id=1, source_target_pairs={{0,1},{1,2},{2,3},{3,0},{4,5},{5,6},{6,7},{7,4},{8,9},{9,10},{10,1... | collective-permute-start | bytes 393224 | tf_op jit(solution)/shard_map/ppermute | solution.py:51
  65.0 6.5 %collective-permute-start.15 = (bf16[64,1024]{1,0:T(8,128)(2,1)S(1)}, bf16[64,1024]{1,0:T(8,128)(2,1)S(1)}, u32[]{:S(2)}, u32[]{:S(2)}) collective-permute-start(bf16[64,1024]{1,0:T(8,128)(2,1)S(1)} %get-tuple-element.52), channel_id=1, source_target_pairs={{0,2},{1,3},{2,0},{3,1},{4,6},{5,7},{6,4},{7,5},{8,10},{9,11},{10,... | collective-permute-start | bytes 393224 | tf_op jit(solution)/shard_map/ppermute | solution.py:51
  65.3 6.1 %collective-permute-start.16 = (bf16[64,1024]{1,0:T(8,128)(2,1)S(1)}, bf16[64,1024]{1,0:T(8,128)(2,1)S(1)}, u32[]{:S(2)}, u32[]{:S(2)}) collective-permute-start(bf16[64,1024]{1,0:T(8,128)(2,1)S(1)} %get-tuple-element.53), channel_id=1, source_target_pairs={{0,3},{1,0},{2,1},{3,2},{4,7},{5,4},{6,5},{7,6},{8,11},{9,8},{10,9... | collective-permute-start | bytes 393224 | tf_op jit(solution)/shard_map/ppermute | solution.py:51
  67.9 12.3 %copy-start.4 = (f32[512]{0:T(512)S(1)}, f32[512]{0:T(512)}, u32[]{:S(2)}) copy-start(f32[512]{0:T(512)} %param.33) | copy-start | bytes 6148
  71.7 4.9 %collective-permute-start.19 = (f32[8,64]{1,0:T(8,128)S(1)}, f32[8,64]{1,0:T(8,128)S(1)}, u32[]{:S(2)}, u32[]{:S(2)}) collective-permute-start(f32[8,64]{1,0:T(8,128)S(1)} %get-tuple-element.58.s0), channel_id=1, source_target_pairs={{0,3},{1,0},{2,1},{3,2},{4,7},{5,4},{6,5},{7,6},{8,11},{9,8},{10,9... | collective-permute-start | bytes 6152 | tf_op jit(solution)/shard_map/ppermute | solution.py:51
  73.1 5.1 %collective-permute-start.18 = (f32[8,64]{1,0:T(8,128)S(1)}, f32[8,64]{1,0:T(8,128)S(1)}, u32[]{:S(2)}, u32[]{:S(2)}) collective-permute-start(f32[8,64]{1,0:T(8,128)S(1)} %get-tuple-element.58.s0), channel_id=1, source_target_pairs={{0,2},{1,3},{2,0},{3,1},{4,6},{5,7},{6,4},{7,5},{8,10},{9,11},{10,... | collective-permute-start | bytes 6152 | tf_op jit(solution)/shard_map/ppermute | solution.py:51
  76.6 3.6 %collective-permute-start.17 = (f32[8,64]{1,0:T(8,128)S(1)}, f32[8,64]{1,0:T(8,128)S(1)}, u32[]{:S(2)}, u32[]{:S(2)}) collective-permute-start(f32[8,64]{1,0:T(8,128)S(1)} %get-tuple-element.58.s0), channel_id=1, source_target_pairs={{0,1},{1,2},{2,3},{3,0},{4,5},{5,6},{6,7},{7,4},{8,9},{9,10},{10,1... | collective-permute-start | bytes 6152 | tf_op jit(solution)/shard_map/ppermute | solution.py:51
